TPU v7x, 32 devices: a whole 2x2x4 slice. The times are simulated.
32 devices in a mesh: sp: 4 (over z), fs: 4 (over y, x), tp: 2 (over core).
Axes of the slice: x: 2, y: 2, z: 4, core: 2. Of those that a mesh axis runs over, the one named last changes fastest.
Arguments:
- tokens: bfloat16 [4, 1024, 2048], P('fs', 'sp', 'tp'), may hold values from -6 to 6
- norm_gain: float32 [2048], replicated, may hold values from 0.1 to 1.9
- w_query: bfloat16 [2048, 1024], P(('sp', 'fs'), 'tp'), may hold values from -0.125 to 0.125
- forget_weight: bfloat16 [2048, 1024], P(('sp', 'fs'), 'tp'), may hold values from -0.125 to 0.125
- w_input: bfloat16 [2048, 1024], P(('sp', 'fs'), 'tp'), may hold values from -8 to 8
- w_outgate: bfloat16 [2048, 1024], P(('sp', 'fs'), 'tp'), may hold values from -0.125 to 0.125
- w_pool: bfloat16 [2048, 1024], P(('sp', 'fs'), 'tp'), may hold values from -0.125 to 0.125
- forget_gap: float32 [1024], P('tp'), may hold values from 0 to 0.07
- extra_decay: float32 [4, 1024, 8], P('fs', 'sp', 'tp'), may hold values from -0.61 to 0
- rec_gain: float32 [1024], P('tp'), may hold values from 0.1 to 1.9
- group_weight: bfloat16 [4, 256, 256], replicated, may hold values from -0.375 to 0.375
- pool_gain: float32 [1024], P('tp'), may hold values from 0.1 to 1.9
- recurrent_output_weight: bfloat16 [1024, 2048], P('tp', ('sp', 'fs')), may hold values from -0.1875 to 0.1875
- w_out_pool: bfloat16 [1024, 2048], P('tp', ('sp', 'fs')), may hold values from -0.1875 to 0.1875
Outputs:
- mixed_out: bfloat16 [4, 1024, 2048], P('fs', ('sp', 'tp'))
All inputs are finite; a program needn't handle non-finite values.
Results may differ from a plain program's by a relative error of at most 0.011.
Values may be sent and summed in bfloat16 or wider, within the bound.
A program may use at most 64 MiB of HBM per device.

v0:
```python
import functools
import jax
import jax.numpy as jnp
from jax import lax
from jax.experimental import pallas as pl
from jax.experimental.pallas import tpu as pltpu
from jax.sharding import PartitionSpec as P

HEAD_DIM = 128
POOL_GROUPS = 4
BLOCK = 64
EPS = 1e-06
HIGH = lax.Precision.HIGHEST
MESH = pl.DeviceIdType.MESH
BF = jnp.bfloat16
F32 = jnp.float32


def place():
    return lax.axis_index("sp"), lax.axis_index("fs"), lax.axis_index("tp")


def rcopy(src, dst, ssem, rsem, dev):
    return pltpu.make_async_remote_copy(
        src_ref=src, dst_ref=dst, send_sem=ssem, recv_sem=rsem, device_id=dev, device_id_type=MESH
    )


def greet(devs):
    barrier = pltpu.get_barrier_semaphore()
    for cond, dev in devs:
        def tell(dev=dev):
            pl.semaphore_signal(barrier, inc=1, device_id=dev, device_id_type=MESH)
        if cond is None:
            tell()
        else:
            pl.when(cond)(tell)
    pl.semaphore_wait(barrier, sum(1 if cond is None else jnp.where(cond, 1, 0) for cond, _ in devs))


def square(f):
    near = f + 1 - 2 * lax.rem(f, 2)
    return near, lax.rem(f + 2, 4), lax.rem(near + 2, 4)


def project_kernel(
    n_sp, n_fs, n_tp, tok, wq, wf, wi, wo, wp, extra, gain, gmap, pgain, wor, wop, z_ref, e_ref, ow_ref,
    wsrc, xs, ws, acc, x_send, x_recv, f_send, d_send, d_recv, w_send, w_recv, zr_send, zl_send, e_send, e_recv,
):
    s, f, t = place()
    rows, half = tok.shape
    part = rows // 2
    mats = (wq, wf, wi, wo, wp)
    wr, width = wq.shape
    ch = width // n_fs
    for i, w in enumerate(mats):
        for g in range(n_fs):
            wsrc[g, :, i * ch : (i + 1) * ch] = w[:, g * ch : (g + 1) * ch]
    other = (s, f, 1 - t)
    px, py, pd = square(f)
    order = (f, px, py, pd)
    up, down = (s + 1, f, t), (s - 1, f, t)
    has_up, has_down = s < n_sp - 1, s > 0
    greet([(None, other)] + [(None, (s, g, t)) for g in order[1:]] + [(has_up, up), (has_down, down)])

    def cols(c):
        return pl.ds(pl.multiple_of(c * half, half), half)

    def span(a, b):
        return pl.ds(pl.multiple_of((a * n_fs + b) * wr, wr), wr)

    def slot(a, b):
        return ws.at[span(a, b), :]

    def to_up(src, a, b):
        return rcopy(src, slot(a, b), zr_send.at[a, b], w_recv.at[a, b], up)

    def to_down(src, a, b):
        return rcopy(src, slot(a, b), zl_send.at[a, b], w_recv.at[a, b], down)

    sends = []

    def send(c):
        c.start()
        sends.append(c)

    def x_slot(g, h, c):
        return xs.at[g, h * part : (h + 1) * part, cols(c)]

    own = wsrc.at[f]
    pl.when(has_up)(lambda: to_up(own, s, f).start())
    pl.when(has_down)(lambda: to_down(own, s, f).start())
    for i, g in enumerate((pd, px, py)):
        send(rcopy(wsrc.at[g], slot(s, f), w_send.at[i], w_recv.at[s, f], (s, g, t)))
    for i, (p, hs) in enumerate(((px, (0, 1)), (py, (1, 0)))):
        for h in hs:
            send(rcopy(tok.at[h * part : (h + 1) * part, :], x_slot(f, h, t), x_send.at[i, h], x_recv.at[f, h], (s, p, t)))
    for h in range(2):
        send(rcopy(tok.at[h * part : (h + 1) * part, :], x_slot(f, h, t), d_send.at[f, h], d_recv.at[f, h], other))
    for i, g in enumerate(order[1:]):
        send(rcopy(extra.at[g], e_ref.at[f], e_send.at[i], e_recv.at[f], (s, g, t)))
    ws[span(s, f), :] = wsrc[f]
    xs[f, :, cols(t)] = tok[...]
    e_ref[f] = extra[f]
    ow_ref[0:width, :] = wor[...]
    gd = gmap.shape[1]
    for i in range(width // gd):
        at = slice(i * gd, (i + 1) * gd)
        scaled = (gmap[t * (width // gd) + i].astype(F32) * pgain[:, at]).astype(BF)
        folded = jnp.dot(scaled, wop[at, :], preferred_element_type=F32)
        ow_ref[width + i * gd : width + (i + 1) * gd, :] = folded.astype(BF)

    for g in order[1:]:
        to_up(slot(s, g), s, g).wait_recv()
        pl.when(has_up)(lambda: to_up(slot(s, g), s, g).start())
        pl.when(has_down)(lambda: to_down(slot(s, g), s, g).start())

    def landed(g, h):
        here = x_slot(g, h, t)
        rcopy(here, here, d_send.at[g, h], x_recv.at[g, h], other).wait_recv()
        return here

    def hand_on(g, h, here):
        send(rcopy(here, here, d_send.at[g, h], d_recv.at[g, h], other))

    for i, (g, h, onto) in enumerate(((px, 0, py), (py, 1, px))):
        here = landed(g, h)
        send(rcopy(here, here, f_send.at[i], x_recv.at[g, h], (s, onto, t)))
        hand_on(g, h, here)

    def relay(d):
        for g in order:
            a = s - d

            @pl.when(a >= 0)
            def _():
                to_up(slot(a, g), a, g).wait_recv()
                pl.when(has_up)(lambda: to_up(slot(a, g), a, g).start())
            b = s + d

            @pl.when(b < n_sp)
            def _():
                to_down(slot(b, g), b, g).wait_recv()
                pl.when(has_down)(lambda: to_down(slot(b, g), b, g).start())

    def add(a):
        k = pl.ds(pl.multiple_of(a * n_fs * wr, n_fs * wr), n_fs * wr)

        def each(i, _):
            acc[i] += jnp.dot(xs[i, :, k], ws[k, :], preferred_element_type=F32)
            return 0

        lax.fori_loop(0, n_fs, each, 0)

    def multiply(d):
        pl.when(s - d >= 0)(lambda: add(s - d))
        pl.when(s + d < n_sp)(lambda: add(s + d))

    relay(1)
    for g, h in ((px, 1), (py, 0), (pd, 0), (pd, 1)):
        hand_on(g, h, landed(g, h))
    for d in range(2, n_sp - 1):
        relay(d)
    for g in order:
        for h in range(2):
            here = x_slot(g, h, 1 - t)
            rcopy(here, here, d_send.at[g, h], d_recv.at[g, h], other).wait_recv()
    for g in order[1:]:
        rcopy(extra.at[f], e_ref.at[g], e_send.at[0], e_recv.at[g], other).wait_recv()
    for c in sends:
        c.wait_send()

    def norm(j, _):
        tile = 16
        per = rows // tile
        at = (j // per, pl.ds(pl.multiple_of(lax.rem(j, per) * tile, tile), tile))
        feats = xs[at[0], at[1], :].astype(F32)
        scale = lax.rsqrt(jnp.mean(feats * feats, axis=-1, keepdims=True) + EPS)
        xs[at[0], at[1], :] = (feats * scale * gain[...]).astype(BF)
        return 0

    lax.fori_loop(0, n_fs * rows // 16, norm, 0, unroll=2)

    if n_fs * wr % 128 == 0:
        own_k = pl.ds(pl.multiple_of(s * n_fs * wr, n_fs * wr), n_fs * wr)

        def begin(i, _):
            acc[i] = jnp.dot(xs[i, :, own_k], ws[own_k, :], preferred_element_type=F32)
            return 0

        lax.fori_loop(0, n_fs, begin, 0)
        for d in range(1, n_sp - 1):
            multiply(d)
        relay(n_sp - 1)
        multiply(n_sp - 1)

        def finish(i, _):
            z_ref[i] = acc[i].astype(BF)
            return 0
    else:
        relay(n_sp - 1)

        def finish(i, _):
            z_ref[i] = jnp.dot(xs[i], ws[...], preferred_element_type=F32).astype(BF)
            return 0

    lax.fori_loop(0, n_fs, finish, 0)

    for d in range(n_sp):
        for g in order:
            a = s - d

            @pl.when((a >= 0) & has_up)
            def _():
                to_up(slot(a, g), a, g).wait_send()
            b = s + d

            @pl.when((b < n_sp) & has_down)
            def _():
                to_down(slot(b, g), b, g).wait_send()


def dot(a, b, dims):
    return lax.dot_general(a, b, (dims, ((), ())), precision=HIGH, preferred_element_type=F32)


def state_kernel(
    n_sp, group_dim, z, e_all, gap, rec_gain, act, sq_out,
    local, qd, own_st, own_de, st_in, de_in, rim, s_send, s_recv, c_send, c_recv, g_send, g_recv,
):
    s, f, t = place()
    n_fs, rows, _ = z.shape
    ch = HEAD_DIM
    reach = rim.shape[1]
    devs = []
    for d in range(1, n_sp):
        devs.append((s + d < n_sp, (s + d, f, t)))
        devs.append((s - d >= 0, (s - d, f, t)))
    greet(devs)
    edge = rcopy(z.at[:, rows - reach :, 4 * ch :], rim, g_send, g_recv, (s + 1, f, t))
    pl.when(s < n_sp - 1)(edge.start)
    mine = pl.ds(pl.multiple_of(f * ch, ch), ch)
    gap_f = gap[:, mine]
    gain_f = rec_gain[:, mine]
    at = lax.broadcasted_iota(jnp.int32, (BLOCK, BLOCK), 0)
    causal = at >= lax.broadcasted_iota(jnp.int32, (BLOCK, BLOCK), 1)
    lower = causal.astype(F32)

    def one(g, _):
        state = jnp.zeros((ch, ch), F32)
        so_far = jnp.zeros((1, ch), F32)
        e_cols = e_all[g].T
        for n in range(rows // BLOCK):
            here = slice(n * BLOCK, (n + 1) * BLOCK)
            q, fo, v = (z[g, here, i * ch : (i + 1) * ch].astype(F32) for i in range(3))
            q = jax.nn.silu(q)
            k = gap_f * jax.nn.sigmoid(-fo)
            lo = n * BLOCK % 128
            lane = n * BLOCK // 128
            logs = jnp.log1p(-k) + e_cols[lo : lo + BLOCK, lane : lane + 1]
            within = dot(lower, logs, ((1,), (0,)))
            end = within[BLOCK - 1 :]
            q_up = q * jnp.exp(within)
            scores = jnp.where(causal, dot(q_up, k * jnp.exp(-within), ((1,), (1,))), 0.0)
            out = dot(scores, v, ((1,), (0,)))
            if n:
                out = out + dot(q_up, state, ((1,), (1,)))
            local[g, here, :] = out
            qd[g, here, :] = q_up * jnp.exp(so_far)
            state = state * jnp.exp(end) + dot(v.T, k * jnp.exp(end - within), ((1,), (0,)))
            so_far = so_far + end
        own_st[g] = state.astype(BF)
        own_de[g] = jnp.broadcast_to(jnp.exp(so_far), (8, ch))
        return 0

    lax.fori_loop(0, n_fs, one, 0)

    def pair(d):
        dev = (s + d, f, t)
        return (
            rcopy(own_st, st_in.at[d - 1], s_send.at[d - 1], s_recv.at[d - 1], dev),
            rcopy(own_de, de_in.at[d - 1], c_send.at[d - 1], c_recv.at[d - 1], dev),
        )

    for d in range(1, n_sp):
        @pl.when(s + d < n_sp)
        def _():
            for c in pair(d):
                c.start()

        @pl.when(s - d < 0)
        def _():
            st_in[d - 1] = jnp.zeros(st_in.shape[1:], st_in.dtype)
            de_in[d - 1] = jnp.ones(de_in.shape[1:], de_in.dtype)
    pl.when(s == 0)(lambda: rim.__setitem__(Ellipsis, jnp.zeros(rim.shape, rim.dtype)))
    pl.when(s > 0)(edge.wait_recv)
    group = (t * n_fs * ch + f * ch) // group_dim
    spot = s * rows + lax.broadcasted_iota(jnp.int32, (rows, ch), 0)
    window = 2
    for level in range(1, POOL_GROUPS):
        window = jnp.where(group == level, 2 ** (level + 1), window)
    counts = jnp.minimum(spot + 1, window).astype(F32)
    for g in range(n_fs):
        zp = z[g, :, 4 * ch :].astype(F32)
        running = jnp.concatenate([rim[g].astype(F32), zp], axis=0)
        total = None
        for level in range(POOL_GROUPS):
            stride = 2**level
            running = running[stride:] + running[:-stride]
            now = running[running.shape[0] - rows :]
            total = now if level == 0 else jnp.where(group == level, now, total)
        act[1, g * rows : (g + 1) * rows, :] = (total / counts - zp).astype(BF)
    for d in range(1, n_sp):
        @pl.when(s - d >= 0)
        def _():
            for c in pair(d):
                c.wait_recv()

    ones = jnp.ones((8, ch), F32)

    def finish(g, _):
        total = jnp.zeros((ch, ch), F32)
        for d in range(n_sp - 2, -1, -1):
            total = de_in[d, g, 0:1, :] * total + st_in[d, g].astype(F32)
        rec = local[g] + dot(qd[g], total, ((1,), (1,)))
        sums = dot(ones, rec * rec, ((1,), (1,)))
        for i in range(rows // 128):
            sq_out[g, i : i + 1, :] = sums[0:1, i * 128 : (i + 1) * 128]
        gate = jax.nn.silu(z[g, :, 3 * ch : 4 * ch].astype(F32))
        act[0, pl.ds(pl.multiple_of(g * rows, rows), rows), :] = (rec * gain_f * gate).astype(BF)
        return 0

    sq_out[...] = jnp.zeros(sq_out.shape, F32)
    lax.fori_loop(0, n_fs, finish, 0)
    for d in range(1, n_sp):
        @pl.when(s + d < n_sp)
        def _():
            for c in pair(d):
                c.wait_send()
    pl.when(s < n_sp - 1)(edge.wait_send)


def mix_kernel(
    n_sp, n_fs, n_tp, act, sq, ow, final,
    out, acts, sq_all, ow_all, relay_buf, wbuf, part,
    a_send, a_recv, f_send, d_send, d_recv, q_send, q_recv,
    up_send, down_send, o_recv, od_send, od_recv, m_send, m_recv,
):
    s, f, t = place()
    n_half = n_sp // n_tp
    rows = act.shape[1] // n_fs
    half = rows // n_tp
    width, cw = ow.shape[0] // 2, ow.shape[1]
    other = (s, f, 1 - t)
    px, py, pd = square(f)
    up, down = (s + 1, f, t), (s - 1, f, t)
    has_up, has_down = s < n_sp - 1, s > 0
    greet(
        [(None, other)]
        + [(None, (s, g, u)) for g in (px, py, pd) for u in (t, 1 - t)]
        + [(has_up, up), (has_down, down)]
    )

    def to_up(src, a):
        return rcopy(src, relay_buf.at[a], up_send.at[a], o_recv.at[a], up)

    def to_down(src, a):
        return rcopy(src, relay_buf.at[a], down_send.at[a], o_recv.at[a], down)

    def to_other(src, a):
        return rcopy(src, ow_all.at[lax.rem(a, n_half), t], od_send.at[a], od_recv.at[a], other)

    def keep(src, a):
        mine = a // n_half == t

        @pl.when(mine)
        def _():
            ow_all[lax.rem(a, n_half), t] = src[...]

        pl.when(jnp.logical_not(mine))(lambda: to_other(src, a).start())

    sends = []

    def send(c):
        c.start()
        sends.append(c)

    for i, (p, order) in enumerate(((px, (0, 1)), (py, (1, 0)))):
        for h in order:
            send(rcopy(act.at[h], acts.at[t, f, h], a_send.at[i, h], a_recv.at[f, h], (s, p, t)))
    pl.when(has_up)(lambda: to_up(ow, s).start())
    pl.when(has_down)(lambda: to_down(ow, s).start())
    for h in range(2):
        send(rcopy(act.at[h], acts.at[t, f, h], d_send.at[f, h], d_recv.at[f, h], other))
    for i, g in enumerate((px, py, pd)):
        for u in range(n_tp):
            send(rcopy(sq, sq_all.at[t, f], q_send.at[i, u], q_recv.at[t, f], (s, g, u)))
    send(rcopy(sq, sq_all.at[t, f], q_send.at[n_fs - 1, 0], q_recv.at[t, f], other))
    acts[t, f] = act[...]
    sq_all[t, f] = sq[...]
    keep(ow, s)

    def landed(g, h):
        here = acts.at[t, g, h]
        rcopy(here, here, d_send.at[g, h], a_recv.at[g, h], other).wait_recv()
        return here

    def hand_on(g, h, here):
        send(rcopy(here, here, d_send.at[g, h], d_recv.at[g, h], other))

    for i, (g, h, onto) in enumerate(((px, 0, py), (py, 1, px))):
        here = landed(g, h)
        send(rcopy(here, here, f_send.at[i], a_recv.at[g, h], (s, onto, t)))
        hand_on(g, h, here)

    def step(d):
        a = s - d

        @pl.when(a >= 0)
        def _():
            to_up(relay_buf.at[a], a).wait_recv()
            pl.when(has_up)(lambda: to_up(relay_buf.at[a], a).start())
            keep(relay_buf.at[a], a)
        b = s + d

        @pl.when(b < n_sp)
        def _():
            to_down(relay_buf.at[b], b).wait_recv()
            pl.when(has_down)(lambda: to_down(relay_buf.at[b], b).start())
            keep(relay_buf.at[b], b)

    for d in range(1, n_sp):
        step(d)
    for g, h in ((px, 1), (py, 0), (pd, 0), (pd, 1)):
        hand_on(g, h, landed(g, h))
    for i in range(n_half):
        a = t * n_half + i
        here = ow_all.at[i, 1 - t]
        rcopy(here, here, od_send.at[a], od_recv.at[a], other).wait_recv()
    for i in range(n_half):
        for u in range(n_tp):
            for k in range(2):
                wbuf[k, u * width : (u + 1) * width, i * cw : (i + 1) * cw] = ow_all[i, u, k * width : (k + 1) * width, :]
    for g in (px, py, pd):
        for u in range(n_tp):
            here = sq_all.at[u, g]
            rcopy(here, here, q_send.at[0, 0], q_recv.at[u, g], other).wait_recv()
    here = sq_all.at[1 - t, f]
    rcopy(here, here, q_send.at[0, 0], q_recv.at[1 - t, f], other).wait_recv()
    for g in (f, px, py, pd):
        for h in range(2):
            here = acts.at[1 - t, g, h]
            rcopy(here, here, d_send.at[g, h], d_recv.at[g, h], other).wait_recv()

    def piece(g, u):
        return rcopy(part.at[g, u], out.at[f, t], m_send.at[g, u], m_recv.at[f, t], (s, g, u))

    def spread(g):
        for u in range(n_tp):
            c = piece(g, u)
            c.start()
            sends.append(c)

    last = None
    for g in (pd, f, px, py):
        here = pl.ds(pl.multiple_of(g * rows, rows), rows)
        sums = sum(sq_all[u, i, g] for u in range(n_tp) for i in range(n_fs))
        scale = lax.rsqrt(sums / (n_tp * width) + EPS).T
        scale = jnp.concatenate([scale[:, i : i + 1] for i in range(rows // 128)], axis=0)
        left = [
            jnp.concatenate([acts[u, i, h, here, :] for u in range(n_tp) for i in range(n_fs)], axis=1)
            for h in range(2)
        ]
        mixed = (
            jnp.dot(left[0], wbuf[0], preferred_element_type=F32) * scale
            + jnp.dot(left[1], wbuf[1], preferred_element_type=F32)
        ).astype(BF)
        for u in range(n_tp):
            part[g, u] = mixed[u * half : (u + 1) * half]
        if last is not None and last is not f:
            spread(last)
        if last is f:
            c = piece(f, 1 - t)
            c.start()
            sends.append(c)
        last = g
    out[f, t] = part[f, t]
    for i in range(n_half):
        to_other(ow, (1 - t) * n_half + i).wait_send()
    for d in range(n_sp):
        a, b = s - d, s + d

        @pl.when((a >= 0) & has_up)
        def _():
            to_up(ow, a).wait_send()

        @pl.when((b < n_sp) & has_down)
        def _():
            to_down(ow, b).wait_send()
    spread(last)
    for c in sends:
        c.wait_send()
    for g in (px, py, pd):
        for u in range(n_tp):
            here = out.at[g, u]
            rcopy(here, here, m_send.at[g, u], m_recv.at[g, u], other).wait_recv()
    here = out.at[f, 1 - t]
    rcopy(here, here, m_send.at[f, 1 - t], m_recv.at[f, 1 - t], other).wait_recv()
    for u in range(n_tp):
        for i in range(n_half):
            for g in range(n_fs):
                lo = ((u * n_half + i) * n_fs + g) * cw
                final[:, lo : lo + cw] = out[g, u, :, i * cw : (i + 1) * cw]


def vmem(count):
    return [pl.BlockSpec(memory_space=pltpu.VMEM)] * count


def dma(*shape):
    return pltpu.SemaphoreType.DMA(shape) if shape else pltpu.SemaphoreType.DMA


def comm(kernel, outs, scratch, number, name):
    return pl.pallas_call(
        kernel,
        out_shape=[jax.ShapeDtypeStruct(a, b) for a, b in outs],
        out_specs=vmem(len(outs)),
        scratch_shapes=scratch,
        compiler_params=pltpu.CompilerParams(
            collective_id=number, has_side_effects=True, vmem_limit_bytes=60 * 1024 * 1024
        ),
        name=name,
    )


def body(
    n_sp, n_fs, n_tp, tokens, norm_gain, w_query, forget_weight, w_input, w_outgate, w_pool, forget_gap,
    extra_decay, rec_gain, group_weight, pool_gain, recurrent_output_weight, w_out_pool,
):
    s, f, t = place()
    rows, half = tokens.shape[1:]
    width = w_query.shape[1]
    ch = width // n_fs
    n_w = 5
    wr = w_query.shape[0]
    lanes = rows // 128
    extra = jnp.pad(extra_decay[0].T.reshape(n_fs, lanes, 128), ((0, 0), (0, 8 - lanes), (0, 0)))
    cw = w_out_pool.shape[1]
    z, e_all, ow = comm(
        functools.partial(project_kernel, n_sp, n_fs, n_tp),
        [((n_fs, rows, n_w * ch), BF), ((n_fs, 8, 128), F32), ((2 * width, cw), BF)],
        [
            pltpu.VMEM((n_fs, wr, n_w * ch), BF), pltpu.VMEM((n_fs, rows, n_tp * half), BF),
            pltpu.VMEM((n_sp * n_fs * wr, n_w * ch), BF), pltpu.VMEM((n_fs, rows, n_w * ch), F32),
            dma(2, 2), dma(n_fs, 2), dma(2), dma(n_fs, 2), dma(n_fs, 2), dma(n_fs - 1), dma(n_sp, n_fs),
            dma(n_sp, n_fs), dma(n_sp, n_fs), dma(n_fs - 1), dma(n_fs),
        ],
        1, "project",
    )(
        tokens[0], w_query, forget_weight, w_input, w_outgate, w_pool, extra, norm_gain[None],
        group_weight, pool_gain[None], recurrent_output_weight, w_out_pool,
    )
    n_half = n_sp // n_tp
    act, sq = comm(
        functools.partial(state_kernel, n_sp, group_weight.shape[1]),
        [((2, n_fs * rows, ch), BF), ((n_fs, 8, 128), F32)],
        [
            pltpu.VMEM((n_fs, rows, ch), F32), pltpu.VMEM((n_fs, rows, ch), F32),
            pltpu.VMEM((n_fs, ch, ch), BF), pltpu.VMEM((n_fs, 8, ch), F32),
            pltpu.VMEM((n_sp - 1, n_fs, ch, ch), BF), pltpu.VMEM((n_sp - 1, n_fs, 8, ch), F32),
            pltpu.VMEM((n_fs, 2**POOL_GROUPS, ch), BF),
            dma(n_sp - 1), dma(n_sp - 1), dma(n_sp - 1), dma(n_sp - 1), dma(), dma(),
        ],
        2, "state",
    )(z, e_all, forget_gap[None], rec_gain[None])
    out_shape = (n_fs, n_tp, rows // n_tp, n_half * cw)
    (final,) = comm(
        functools.partial(mix_kernel, n_sp, n_fs, n_tp),
        [((rows // n_tp, n_tp * n_half * n_fs * cw), BF)],
        [
            pltpu.VMEM(out_shape, BF), pltpu.VMEM((n_tp, n_fs) + act.shape, BF), pltpu.VMEM((n_tp, n_fs) + sq.shape, F32),
            pltpu.VMEM((n_half, n_tp) + ow.shape, BF), pltpu.VMEM((n_sp,) + ow.shape, BF),
            pltpu.VMEM((2, n_tp * width, n_half * cw), BF), pltpu.VMEM(out_shape, BF),
            dma(2, 2), dma(n_fs, 2), dma(2), dma(n_fs, 2), dma(n_fs, 2), dma(n_fs, n_tp), dma(n_tp, n_fs),
            dma(n_sp), dma(n_sp), dma(n_sp), dma(n_sp), dma(n_sp), dma(n_fs, n_tp), dma(n_fs, n_tp),
        ],
        3, "mix",
    )(act, sq, ow)
    return final[None]


def solution(mesh):
    sizes = dict(mesh.shape)
    weight = P(("sp", "fs"), "tp")
    placed = (
        P("fs", "sp", "tp"), P(), weight, weight, weight, weight, weight, P("tp"),
        P("fs", "sp", "tp"), P("tp"), P(), P("tp"), P("tp", ("sp", "fs")), P("tp", ("sp", "fs")),
    )
    return jax.shard_map(
        functools.partial(body, sizes["sp"], sizes["fs"], sizes["tp"]),
        mesh=mesh, in_specs=placed, out_specs=P("fs", ("sp", "tp"), None), check_vma=False,
    )
```

profile of v0, /device:TPU:1, one launch (start us, length us, event | category | flops | bytes accessed | tf_op | source)
XLA Modules:
  0.0 122.1 jit_solution(12853854571828597920)
XLA Ops:
  0.0 0.7 reshape.3
  0.7 0.6 pad.4.extra
  1.3 54.3 %project.1 = (bf16[4,256,640]{2,1,0:T(8,128)(2,1)}, f32[4,8,128]{2,1,0:T(8,128)}, bf16[1024,128]{1,0:T(8,128)(2,1)}) custom-call(bf16[256,1024]{1,0:T(8,128)(2,1)} %bitcast.10, bf16[128,512]{1,0:T(8,128)(2,1)} %wq.1, bf16[128,512]{1,0:T(8,128)(2,1)} %wf.1, bf16[128,512]{1,0:T(8,128)(2,1)} %wi.1, bf16[128,512]{1,0:T(8,128)(2,1)} %wo.1, bf16[128,512]{1,0:T(8,128)(2,1)} %wp.1, ...), custom_call_target="tpu_custom_call" | custom-call | tf_op jit(solution)/shard_map/project/pallas_call | solution.py:550
  55.6 17.9 %state.1 = (bf16[2,1024,128]{2,1,0:T(8,128)(2,1)}, f32[4,8,128]{2,1,0:T(8,128)}) custom-call(bf16[4,256,640]{2,1,0:T(8,128)(2,1)} %get-tuple-element.10.z, f32[4,8,128]{2,1,0:T(8,128)} %get-tuple-element.11.e_all, f32[1,512]{1,0:T(1,128)} %bitcast.14, f32[1,512]{1,0:T(1,128)} %bitcast.15), custom_call_target="tpu_custom_call" | custom-call | tf_op jit(solution)/shard_map/state/pallas_call | solution.py:565
  73.5 46.7 %mix.1 = bf16[128,2048]{1,0:T(8,128)(2,1)} custom-call(bf16[2,1024,128]{2,1,0:T(8,128)(2,1)} %get-tuple-element.12.act, f32[4,8,128]{2,1,0:T(8,128)} %get-tuple-element.13.sq, bf16[1024,128]{1,0:T(8,128)(2,1)} %get-tuple-element.14.ow), custom_call_target="tpu_custom_call" | custom-call | tf_op jit(solution)/shard_map/mix/pallas_call | solution.py:578
  120.2 1.9 %copy.16 = bf16[1,128,2048]{2,1,0:T(8,128)(2,1)} copy(bf16[1,128,2048]{2,1,0:T(8,128)(2,1)} %bitcast.9) | data formatting | bytes 1048576
where the time goes:
time: 122 us
  Pallas kernels  119 us (98%)
  local copies, waits for them, and re-layouts  3.19 us (3%)
    pallas_call x1, Pallas kernels, body(): comm(functools.partial(project_kernel, n_sp, n_fs, n_tp), [((n_fs, rows,...  54.3 us
    pallas_call x1, Pallas kernels, body(): comm(functools.partial(mix_kernel, n_sp, n_fs, n_tp), [((rows // n_tp, n_...  46.7 us
    pallas_call x1, Pallas kernels, body(): comm(functools.partial(state_kernel, n_sp, group_weight.shape[1]), [((2,...  17.9 us

commit v1 on v0

--- a/solution.py
+++ b/solution.py
@@ -590,6 +590,596 @@
     return final[None]
 
 
+def mm(a, b, dims):
+    return lax.dot_general(a, b, (dims, ((), ())), preferred_element_type=F32)
+
+
+NN, NT, TN = ((1,), (0,)), ((1,), (1,)), ((0,), (0,))
+
+
+def layer_kernel(
+    n_sp, n_fs, n_tp, tok, wq, wf, wi, wo, wp, extra, gain, gap, rec_gain, gmap, pgain, wor, wop, final,
+    src0, src1, src2, ws0, ws1, ws2, xs, xn, acc0, acc1, acc2, e_src, e_all, local, qd, own_st, own_de,
+    t_out, t_in, rim_src, rim, acts, sq_src, sq_all, ow_buf, ow_oth, part,
+    x_send, x_recv, xf_send, xd_send, xd_recv, w_send, w_recv, up_send, dn_send, e_send, e_recv,
+    t_send, t_recv, g_send, g_recv, a_send, a_recv, af_send, ad_send, ad_recv, q_send, q_recv,
+    ou_send, on_send, o_recv, od_send, od_recv, m_send, m_recv,
+):
+    s, f, t = place()
+    rows, half = tok.shape
+    cut = rows // 2
+    wr, width = wq.shape
+    ch = width // n_fs
+    cw = wor.shape[1]
+    n_half = n_sp // n_tp
+    out_rows = rows // n_tp
+    lanes = rows // 128
+    size = 128
+    groups = ((wq, wf, wi), (wp,), (wo,))
+    srcs, wss, accs = (src0, src1, src2), (ws0, ws1, ws2), (acc0, acc1, acc2)
+    other = (s, f, 1 - t)
+    px, py, pd = square(f)
+    order = (f, px, py, pd)
+    up, down = (s + 1, f, t), (s - 1, f, t)
+    has_up, has_down = s < n_sp - 1, s > 0
+    sends = []
+
+    def send(c):
+        c.start()
+        sends.append(c)
+
+    def when(cond, *copies):
+        @pl.when(cond)
+        def _():
+            for c in copies:
+                c.start()
+
+    def pack(c):
+        for i, w in enumerate(groups[c]):
+            for g in range(n_fs):
+                srcs[c][g, :, i * ch : (i + 1) * ch] = w[:, g * ch : (g + 1) * ch]
+
+    pack(0)
+    e_rows = extra[...].T
+    for g in range(n_fs):
+        e_src[g] = jnp.broadcast_to(e_rows[g : g + 1, :], e_src.shape[1:])
+    greet(
+        [(None, other)]
+        + [(None, (s, g, u)) for g in order[1:] for u in (t, 1 - t)]
+        + [(has_up, up), (has_down, down)]
+    )
+
+    def cols(c):
+        return pl.ds(pl.multiple_of(c * half, half), half)
+
+    def span(a, b):
+        return pl.ds(pl.multiple_of((a * n_fs + b) * wr, wr), wr)
+
+    def slot(c, a, b):
+        return wss[c].at[span(a, b), :]
+
+    def to_up(c, src, a, b):
+        return rcopy(src, slot(c, a, b), up_send.at[c, a, b], w_recv.at[c, a, b], up)
+
+    def to_down(c, src, a, b):
+        return rcopy(src, slot(c, a, b), dn_send.at[c, a, b], w_recv.at[c, a, b], down)
+
+    def both(c, src, a, b):
+        when(has_up, to_up(c, src, a, b))
+        when(has_down, to_down(c, src, a, b))
+
+    def spread(c):
+        for i, g in enumerate(order[1:]):
+            send(rcopy(srcs[c].at[g], slot(c, s, f), w_send.at[c, i], w_recv.at[c, s, f], (s, g, t)))
+
+    def from_square(c, g):
+        to_up(c, slot(c, s, g), s, g).wait_recv()
+        both(c, slot(c, s, g), s, g)
+
+    def relay(c, d, gs):
+        for g in gs:
+            a, b = s - d, s + d
+
+            @pl.when((a >= 0) & has_up)
+            def _():
+                to_up(c, slot(c, a, g), a, g).wait_recv()
+                to_up(c, slot(c, a, g), a, g).start()
+
+            @pl.when((b < n_sp) & has_down)
+            def _():
+                to_down(c, slot(c, b, g), b, g).wait_recv()
+                to_down(c, slot(c, b, g), b, g).start()
+
+    def arrive(c, d):
+        for g in order:
+            a, b = s - d, s + d
+
+            @pl.when((a >= 0) & jnp.logical_not(has_up))
+            def _():
+                to_up(c, slot(c, a, g), a, g).wait_recv()
+
+            @pl.when((b < n_sp) & jnp.logical_not(has_down))
+            def _():
+                to_down(c, slot(c, b, g), b, g).wait_recv()
+
+    def gemm(c, a, first=False):
+        k = pl.ds(pl.multiple_of(a * n_fs * wr, n_fs * wr), n_fs * wr)
+        acc, w = accs[c], wss[c]
+
+        def each(i, _):
+            out = jnp.dot(xn[i, :, k], w[k, :], preferred_element_type=F32)
+            acc[i] = out if first else acc[i] + out
+            return 0
+
+        lax.fori_loop(0, n_fs, each, 0)
+
+    def gemm_at(c, d):
+        pl.when(s - d >= 0)(lambda: gemm(c, s - d))
+        pl.when(s + d < n_sp)(lambda: gemm(c, s + d))
+
+    def x_slot(g, h, c):
+        return xs.at[g, h * cut : (h + 1) * cut, cols(c)]
+
+    def landed(g, h):
+        here = x_slot(g, h, t)
+        rcopy(here, here, xd_send.at[g, h], x_recv.at[g, h], other).wait_recv()
+        return here
+
+    def hand_on(g, h, here):
+        send(rcopy(here, here, xd_send.at[g, h], xd_recv.at[g, h], other))
+
+    def norm(g):
+        for h in range(2):
+            here = x_slot(g, h, 1 - t)
+            rcopy(here, here, xd_send.at[g, h], xd_recv.at[g, h], other).wait_recv()
+        tile = 16
+
+        def each(j, _):
+            at = pl.ds(pl.multiple_of(j * tile, tile), tile)
+            feats = xs[g, at, :].astype(F32)
+            scale = lax.rsqrt(jnp.mean(feats * feats, axis=-1, keepdims=True) + EPS)
+            xn[g, at, :] = (feats * scale * gain[...]).astype(BF)
+            return 0
+
+        lax.fori_loop(0, rows // tile, each, 0, unroll=2)
+
+    def ow_up(src, a, k):
+        return rcopy(src, ow_buf.at[a, k], ou_send.at[a, k], o_recv.at[a, k], up)
+
+    def ow_down(src, a, k):
+        return rcopy(src, ow_buf.at[a, k], on_send.at[a, k], o_recv.at[a, k], down)
+
+    def ow_other(a, k):
+        return rcopy(ow_buf.at[a, k], ow_oth.at[lax.rem(a, n_half), k], od_send.at[a, k], od_recv.at[lax.rem(a, n_half), k], other)
+
+    def ow_share(a, k):
+        when(a // n_half != t, ow_other(a, k))
+
+    def ow_relay(d, k):
+        a, b = s - d, s + d
+
+        @pl.when((a >= 0) & has_up)
+        def _():
+            here = ow_buf.at[a, k]
+            ow_up(here, a, k).wait_recv()
+            ow_up(here, a, k).start()
+            ow_share(a, k)
+
+        @pl.when((b < n_sp) & has_down)
+        def _():
+            here = ow_buf.at[b, k]
+            ow_down(here, b, k).wait_recv()
+            ow_down(here, b, k).start()
+            ow_share(b, k)
+
+    def ow_take(d, k):
+        a, b = s - d, s + d
+
+        @pl.when((a >= 0) & jnp.logical_not(has_up))
+        def _():
+            ow_up(ow_buf.at[a, k], a, k).wait_recv()
+            ow_share(a, k)
+
+        @pl.when((b < n_sp) & jnp.logical_not(has_down))
+        def _():
+            ow_down(ow_buf.at[b, k], b, k).wait_recv()
+            ow_share(b, k)
+
+    both(0, src0.at[f], s, f)
+    spread(0)
+    for i, (p, hs) in enumerate(((px, (0, 1)), (py, (1, 0)))):
+        for h in hs:
+            send(rcopy(tok.at[h * cut : (h + 1) * cut, :], x_slot(f, h, t), x_send.at[i, h], x_recv.at[f, h], (s, p, t)))
+    for h in range(2):
+        send(rcopy(tok.at[h * cut : (h + 1) * cut, :], x_slot(f, h, t), xd_send.at[f, h], xd_recv.at[f, h], other))
+    when(has_up, ow_up(wor, s, 0))
+    when(has_down, ow_down(wor, s, 0))
+    for i, g in enumerate(order[1:]):
+        send(rcopy(e_src.at[g], e_all.at[f], e_send.at[i], e_recv.at[f], (s, g, t)))
+    pack(1)
+    pack(2)
+    spread(1)
+    spread(2)
+    for c in range(3):
+        wss[c][span(s, f), :] = srcs[c][f]
+    xs[f, :, cols(t)] = tok[...]
+    e_all[f] = e_src[f]
+    for g in order[1:]:
+        from_square(0, g)
+    ow_buf[s, 0] = wor[...]
+    gd = gmap.shape[1]
+    for i in range(width // gd):
+        at = slice(i * gd, (i + 1) * gd)
+        scaled = (gmap[t * (width // gd) + i].astype(F32) * pgain[:, at]).astype(BF)
+        ow_buf[s, 1, at, :] = jnp.dot(scaled, wop[at, :], preferred_element_type=F32).astype(BF)
+    norm(f)
+    relay(0, 1, order[:2])
+    for i, (g, h, onto) in enumerate(((px, 0, py), (py, 1, px))):
+        here = landed(g, h)
+        send(rcopy(here, here, xf_send.at[i], x_recv.at[g, h], (s, onto, t)))
+        hand_on(g, h, here)
+    relay(0, 1, order[2:])
+    for g, h in ((px, 1), (py, 0)):
+        hand_on(g, h, landed(g, h))
+    for d in range(2, n_sp - 1):
+        relay(0, d, order[:2])
+    norm(px)
+    norm(py)
+    for d in range(2, n_sp - 1):
+        relay(0, d, order[2:])
+    both(1, src1.at[f], s, f)
+    for g in order[1:]:
+        from_square(1, g)
+    for h in range(2):
+        hand_on(pd, h, landed(pd, h))
+    norm(pd)
+
+    for d in range(1, n_sp - 1):
+        arrive(0, d)
+    gemm(0, s, True)
+    for d in range(1, n_sp - 1):
+        gemm_at(0, d)
+    relay(1, 1, order)
+    arrive(0, n_sp - 1)
+    gemm_at(0, n_sp - 1)
+    for g in order[1:]:
+        rcopy(e_src.at[f], e_all.at[g], e_send.at[0], e_recv.at[g], other).wait_recv()
+
+    mine = pl.ds(pl.multiple_of(f * ch, ch), ch)
+    gap_f = gap[:, mine]
+    gain_f = rec_gain[:, mine]
+    at = lax.broadcasted_iota(jnp.int32, (size, size), 0)
+    causal = at >= lax.broadcasted_iota(jnp.int32, (size, size), 1)
+    lower = jnp.where(causal, 1.0, 0.0).astype(BF)
+    lower = jnp.concatenate([lower, lower], axis=1)
+
+    def scan(g):
+        state = None
+        so_far = jnp.zeros((1, ch), F32)
+        e_cols = e_all[g].T
+        for n in range(rows // size):
+            here = slice(n * size, (n + 1) * size)
+            v = acc0[g, here, 2 * ch : 3 * ch].astype(BF)
+            q = jax.nn.silu(acc0[g, here, 0:ch].astype(BF).astype(F32))
+            k = gap_f * jax.nn.sigmoid(-acc0[g, here, ch : 2 * ch].astype(BF).astype(F32))
+            logs = jnp.log1p(-k) + e_cols[here, 0:1]
+            high = logs.astype(BF)
+            low = (logs - high.astype(F32)).astype(BF)
+            within = mm(lower, jnp.concatenate([high, low], axis=0), NN)
+            mid = within[size // 2 - 1 : size // 2]
+            end = within[size - 1 :]
+            q = q * jnp.exp(within - mid)
+            k = (k * jnp.exp(mid - within)).astype(BF)
+            q_up = q.astype(BF)
+            scores = jnp.where(causal, mm(q_up, k, NT), 0.0).astype(BF)
+            out = mm(scores, v, NN)
+            if n:
+                out = out + mm(q_up, (state * jnp.exp(mid)).astype(BF), NT)
+            local[g, here, :] = out
+            qd[g, here, :] = (q * jnp.exp(mid + so_far)).astype(BF)
+            fresh = mm(v, k, TN) * jnp.exp(end - mid)
+            state = state * jnp.exp(end) + fresh if n else fresh
+            so_far = so_far + end
+        own_st[g] = state
+        own_de[g] = jnp.broadcast_to(jnp.exp(so_far), own_de.shape[1:])
+
+    scan(0)
+    scan(1)
+    for d in range(2, n_sp - 1):
+        relay(1, d, order)
+    both(2, src2.at[f], s, f)
+    for g in order[1:]:
+        from_square(2, g)
+    scan(2)
+    scan(3)
+
+    def carry(g):
+        return rcopy(t_out.at[g], t_in.at[g], t_send.at[g], t_recv.at[g], up)
+
+    @pl.when(jnp.logical_not(has_down))
+    def _():
+        t_in[...] = jnp.zeros(t_in.shape, BF)
+        rim[...] = jnp.zeros(rim.shape, BF)
+        t_out[...] = own_st[...].astype(BF)
+        for g in range(n_fs):
+            carry(g).start()
+
+    for d in range(1, n_sp - 1):
+        relay(2, d, order)
+
+    def project(c):
+        gemm(c, s, True)
+        for d in range(1, n_sp - 1):
+            arrive(c, d)
+            gemm_at(c, d)
+        arrive(c, n_sp - 1)
+        gemm_at(c, n_sp - 1)
+
+    project(1)
+    reach = rim.shape[1]
+    rim_src[...] = acc1[:, rows - reach :, :].astype(BF)
+    edge = rcopy(rim_src, rim, g_send, g_recv, up)
+    when(has_up, edge)
+
+    @pl.when(has_down & has_up)
+    def _():
+        for g in range(n_fs):
+            carry(g).wait_recv()
+            t_out[g] = (own_st[g] + t_in[g].astype(F32) * own_de[g, 0:1, :]).astype(BF)
+            carry(g).start()
+
+    when(has_up, ow_up(ow_buf.at[s, 1], s, 1))
+    when(has_down, ow_down(ow_buf.at[s, 1], s, 1))
+    for k in range(2):
+        ow_share(s, k)
+    ow_relay(1, 0)
+    pl.when(has_down)(edge.wait_recv)
+
+    group = (t * n_fs * ch + f * ch) // gd
+    spot = s * rows + lax.broadcasted_iota(jnp.int32, (rows, ch), 0)
+    window = 2
+    for level in range(1, POOL_GROUPS):
+        window = jnp.where(group == level, 2 ** (level + 1), window)
+    share = 1.0 / jnp.minimum(spot + 1, window).astype(F32)
+
+    def pool(g):
+        zp = acc1[g].astype(BF).astype(F32)
+        running = jnp.concatenate([rim[g].astype(F32), zp], axis=0)
+        total = None
+        for level in range(POOL_GROUPS):
+            stride = 2**level
+            running = running[stride:] + running[:-stride]
+            now = running[running.shape[0] - rows :]
+            total = now if level == 0 else jnp.where(group == level, now, total)
+        acts[1, t, f, g * rows : (g + 1) * rows, :] = (total * share - zp).astype(BF)
+
+    part_rows = n_fs * rows // 2
+
+    def a_slot(k, u, g, h):
+        return acts.at[k, u, g, h * part_rows : (h + 1) * part_rows, :]
+
+    def publish(k, h):
+        here = a_slot(k, t, f, h)
+        for i, p in enumerate((px, py)):
+            send(rcopy(here, here, a_send.at[k, i, h], a_recv.at[k, f, h], (s, p, t)))
+        send(rcopy(here, here, ad_send.at[k, f, h], ad_recv.at[k, f, h], other))
+
+    def a_landed(k, g, h):
+        here = a_slot(k, t, g, h)
+        rcopy(here, here, ad_send.at[k, g, h], a_recv.at[k, g, h], other).wait_recv()
+        return here
+
+    def a_hand_on(k, g, h, here):
+        send(rcopy(here, here, ad_send.at[k, g, h], ad_recv.at[k, g, h], other))
+
+    def a_forward(k):
+        for i, (g, h, onto) in enumerate(((px, 0, py), (py, 1, px))):
+            here = a_landed(k, g, h)
+            send(rcopy(here, here, af_send.at[k, i], a_recv.at[k, g, h], (s, onto, t)))
+            a_hand_on(k, g, h, here)
+
+    def a_rest(k):
+        for g, h in ((px, 1), (py, 0), (pd, 0), (pd, 1)):
+            a_hand_on(k, g, h, a_landed(k, g, h))
+
+    def a_other(k):
+        for g in order:
+            for h in range(2):
+                here = a_slot(k, 1 - t, g, h)
+                rcopy(here, here, ad_send.at[k, g, h], ad_recv.at[k, g, h], other).wait_recv()
+
+    for h in range(2):
+        for g in range(h * n_fs // 2, (h + 1) * n_fs // 2):
+            pool(g)
+        publish(1, h)
+    ow_relay(1, 1)
+    for d in range(2, n_sp - 1):
+        ow_relay(d, 0)
+    gemm(2, s, True)
+    for d in range(1, n_sp - 1):
+        arrive(2, d)
+        gemm_at(2, d)
+    a_forward(1)
+    arrive(2, n_sp - 1)
+    gemm_at(2, n_sp - 1)
+
+    @pl.when(has_down & jnp.logical_not(has_up))
+    def _():
+        for g in range(n_fs):
+            carry(g).wait_recv()
+
+    ones = jnp.ones((8, ch), BF)
+
+    def finish(g):
+        rec = local[g] + mm(qd[g], t_in[g], NT)
+        sums = mm(ones, (rec * rec).astype(BF), NT)
+        for i in range(lanes):
+            sq_src[g * lanes + i : g * lanes + i + 1, :] = sums[0:1, i * 128 : (i + 1) * 128]
+        gate = jax.nn.silu(acc2[g].astype(BF).astype(F32))
+        acts[0, t, f, g * rows : (g + 1) * rows, :] = (rec * gain_f * gate).astype(BF)
+
+    for h in range(2):
+        for g in range(h * n_fs // 2, (h + 1) * n_fs // 2):
+            finish(g)
+        publish(0, h)
+    for i, g in enumerate(order[1:]):
+        for u in range(n_tp):
+            send(rcopy(sq_src, sq_all.at[t, f], q_send.at[i, u], q_recv.at[t, f], (s, g, u)))
+    send(rcopy(sq_src, sq_all.at[t, f], q_send.at[n_fs - 1, 0], q_recv.at[t, f], other))
+    sq_all[t, f] = sq_src[...]
+    for d in range(2, n_sp - 1):
+        ow_relay(d, 1)
+    a_rest(1)
+    for k in range(2):
+        ow_take(1, k)
+    a_forward(0)
+    for d in range(2, n_sp - 1):
+        for k in range(2):
+            ow_take(d, k)
+    a_rest(0)
+    a_other(1)
+    a_other(0)
+    for g in order[1:]:
+        for u in range(n_tp):
+            here = sq_all.at[u, g]
+            rcopy(here, here, q_send.at[0, 0], q_recv.at[u, g], other).wait_recv()
+    here = sq_all.at[1 - t, f]
+    rcopy(here, here, q_send.at[0, 0], q_recv.at[1 - t, f], other).wait_recv()
+    sums = sum(sq_all[u, i] for u in range(n_tp) for i in range(n_fs))
+    scale = lax.rsqrt(sums / (n_tp * width) + EPS).T
+    scales = [
+        jnp.concatenate([scale[:, g * lanes + i : g * lanes + i + 1] for i in range(lanes)], axis=0) for g in range(n_fs)
+    ]
+    late = s - t * n_half >= n_half - 1
+
+    def spot_of(a, g):
+        return pl.ds(pl.multiple_of((a * n_fs + g) * cw, cw), cw)
+
+    def piece(i, g, u):
+        return rcopy(
+            part.at[i, g, u], final.at[:, spot_of(t * n_half + i, f)], m_send.at[i, g, u], m_recv.at[i, f, t], (s, g, u)
+        )
+
+    for j in range(n_half):
+        i = jnp.where(late, n_half - 1 - j, j)
+        a = t * n_half + i
+        if j == n_half - 1:
+            for k in range(2):
+                ow_take(n_sp - 1, k)
+        for k in range(2):
+            rcopy(ow_buf.at[a, k], ow_oth.at[i, k], od_send.at[a, k], od_recv.at[i, k], other).wait_recv()
+        for g in range(n_fs):
+            here = pl.ds(g * rows, rows)
+            made = []
+            for k in range(2):
+                total = None
+                for u, w in ((t, ow_buf.at[a, k]), (1 - t, ow_oth.at[i, k])):
+                    left = jnp.concatenate([acts[k, u, b, here, :] for b in range(n_fs)], axis=1)
+                    now = jnp.dot(left, w[...], preferred_element_type=F32)
+                    total = now if total is None else total + now
+                made.append(total)
+            mixed = (made[0] * scales[g] + made[1]).astype(BF)
+            for u in range(n_tp):
+                part[i, g, u] = mixed[u * out_rows : (u + 1) * out_rows]
+                when((g != f) | (u != t), piece(i, g, u))
+        final[:, spot_of(a, f)] = part[i, f, t]
+
+    for i in range(n_half):
+        for g in range(n_fs):
+            for u in range(n_tp):
+                @pl.when((g != f) | (u != t))
+                def _():
+                    here = final.at[:, spot_of(u * n_half + i, g)]
+                    rcopy(here, here, m_send.at[i, g, u], m_recv.at[i, g, u], other).wait_recv()
+                    piece(i, g, u).wait_send()
+    for c in sends:
+        c.wait_send()
+    for c in range(3):
+        for d in range(n_sp):
+            for g in order:
+                a, b = s - d, s + d
+
+                @pl.when((a >= 0) & has_up)
+                def _():
+                    to_up(c, slot(c, a, g), a, g).wait_send()
+
+                @pl.when((b < n_sp) & has_down)
+                def _():
+                    to_down(c, slot(c, b, g), b, g).wait_send()
+    for d in range(n_sp):
+        for k in range(2):
+            a, b = s - d, s + d
+
+            @pl.when((a >= 0) & has_up)
+            def _():
+                ow_up(ow_buf.at[a, k], a, k).wait_send()
+
+            @pl.when((b < n_sp) & has_down)
+            def _():
+                ow_down(ow_buf.at[b, k], b, k).wait_send()
+    for i in range(n_half):
+        for k in range(2):
+            ow_other((1 - t) * n_half + i, k).wait_send()
+
+    @pl.when(has_up)
+    def _():
+        edge.wait_send()
+        for g in range(n_fs):
+            carry(g).wait_send()
+
+
+def fused(
+    n_sp, n_fs, n_tp, tokens, norm_gain, w_query, forget_weight, w_input, w_outgate, w_pool, forget_gap,
+    extra_decay, rec_gain, group_weight, pool_gain, recurrent_output_weight, w_out_pool,
+):
+    rows, half = tokens.shape[1:]
+    wr, width = w_query.shape
+    ch = width // n_fs
+    cw = w_out_pool.shape[1]
+    n_half = n_sp // n_tp
+    feats = n_sp * n_fs * wr
+    lanes = rows // 128
+
+    def buf(kind, *shape):
+        return pltpu.VMEM(shape, kind)
+
+    (final,) = comm(
+        functools.partial(layer_kernel, n_sp, n_fs, n_tp),
+        [((rows // n_tp, n_sp * n_fs * cw), BF)],
+        [
+            buf(BF, n_fs, wr, 3 * ch), buf(BF, n_fs, wr, ch), buf(BF, n_fs, wr, ch),
+            buf(BF, feats, 3 * ch), buf(BF, feats, ch), buf(BF, feats, ch),
+            buf(BF, n_fs, rows, n_tp * half), buf(BF, n_fs, rows, n_tp * half),
+            buf(F32, n_fs, rows, 3 * ch), buf(F32, n_fs, rows, ch), buf(F32, n_fs, rows, ch),
+            buf(F32, n_fs, 8, rows), buf(F32, n_fs, 8, rows),
+            buf(F32, n_fs, rows, ch), buf(BF, n_fs, rows, ch),
+            buf(F32, n_fs, ch, ch), buf(F32, n_fs, 8, ch),
+            buf(BF, n_fs, ch, ch), buf(BF, n_fs, ch, ch),
+            buf(BF, n_fs, 2**POOL_GROUPS, ch), buf(BF, n_fs, 2**POOL_GROUPS, ch),
+            buf(BF, 2, n_tp, n_fs, n_fs * rows, ch),
+            buf(F32, n_fs * lanes, 128), buf(F32, n_tp, n_fs, n_fs * lanes, 128),
+            buf(BF, n_sp, 2, width, cw), buf(BF, n_half, 2, width, cw),
+            buf(BF, n_half, n_fs, n_tp, rows // n_tp, cw),
+            dma(2, 2), dma(n_fs, 2), dma(2), dma(n_fs, 2), dma(n_fs, 2),
+            dma(3, n_fs - 1), dma(3, n_sp, n_fs), dma(3, n_sp, n_fs), dma(3, n_sp, n_fs), dma(n_fs - 1), dma(n_fs),
+            dma(n_fs), dma(n_fs), dma(), dma(),
+            dma(2, 2, 2), dma(2, n_fs, 2), dma(2, 2), dma(2, n_fs, 2), dma(2, n_fs, 2), dma(n_fs, n_tp), dma(n_tp, n_fs),
+            dma(n_sp, 2), dma(n_sp, 2), dma(n_sp, 2), dma(n_sp, 2), dma(n_half, 2), dma(n_half, n_fs, n_tp), dma(n_half, n_fs, n_tp),
+        ],
+        1, "layer",
+    )(
+        tokens[0], w_query, forget_weight, w_input, w_outgate, w_pool, extra_decay[0], norm_gain[None],
+        forget_gap[None], rec_gain[None], group_weight, pool_gain[None], recurrent_output_weight, w_out_pool,
+    )
+    return final[None]
+
+
+def run(n_sp, n_fs, n_tp, *args):
+    wr, width = args[2].shape
+    whole = n_fs * wr % 128 == 0 and args[-1].shape[1] % 128 == 0 and args[0].shape[1] % 256 == 0
+    return (fused if whole and width == n_fs * HEAD_DIM else body)(n_sp, n_fs, n_tp, *args)
+
+
 def solution(mesh):
     sizes = dict(mesh.shape)
     weight = P(("sp", "fs"), "tp")
@@ -598,6 +1188,6 @@
         P("fs", "sp", "tp"), P("tp"), P(), P("tp"), P("tp", ("sp", "fs")), P("tp", ("sp", "fs")),
     )
     return jax.shard_map(
-        functools.partial(body, sizes["sp"], sizes["fs"], sizes["tp"]),
+        functools.partial(run, sizes["sp"], sizes["fs"], sizes["tp"]),
         mesh=mesh, in_specs=placed, out_specs=P("fs", ("sp", "tp"), None), check_vma=False,
     )

time: 122 us -> 98.5 us (0.81)
  the two profiles are of different devices: /device:TPU:1 before, /device:TPU:23 now
where the time goes in v1:
time: 98.5 us; the launch traced here: 98.2 us
  Pallas kernels  94.9 us (96%)
  local copies, waits for them, and re-layouts  3.37 us (3%)
    pallas_call x1, Pallas kernels, fused(): comm(functools.partial(layer_kernel, n_sp, n_fs, n_tp), [((rows // n_tp,...  94.9 us
    unnamed x4, local copies, waits for them, and re-layouts  3.37 us

profile of v1, /device:TPU:23, one launch (start us, length us, event | category | flops | bytes accessed | tf_op | source)
XLA Modules:
  0.0 98.2 jit_solution(7251016857860077690)
XLA Ops:
  0.0 0.0 copy-start
  0.0 0.7 copy-done
  0.7 0.8 copy.15
  1.5 94.9 %layer.1 = bf16[128,2048]{1,0:T(8,128)(2,1)} custom-call(bf16[256,1024]{1,0:T(8,128)(2,1)} %bitcast.9, bf16[128,512]{1,0:T(8,128)(2,1)} %wq.1, bf16[128,512]{1,0:T(8,128)(2,1)} %wf.1, bf16[128,512]{1,0:T(8,128)(2,1)} %wi.1, bf16[128,512]{1,0:T(8,128)(2,1)} %wo.1, bf16[128,512]{1,0:T(8,128)(2,1)} %wp.1, f32[256,4]{1,0:T(8,128)} %bitcast.8, ...), custom_call_target="tpu_custom_call" | custom-call | tf_op jit(solution)/shard_map/layer/pallas_call | solution.py:1146
  96.4 1.9 %copy.17 = bf16[1,128,2048]{2,1,0:T(8,128)(2,1)} copy(bf16[1,128,2048]{2,1,0:T(8,128)(2,1)} %bitcast.7) | data formatting | bytes 1048576
Async XLA Ops:
  0.0 0.7 copy-start

commit v2 on v1

--- a/solution.py
+++ b/solution.py
@@ -600,7 +600,7 @@
 def layer_kernel(
     n_sp, n_fs, n_tp, tok, wq, wf, wi, wo, wp, extra, gain, gap, rec_gain, gmap, pgain, wor, wop, final,
     src0, src1, src2, ws0, ws1, ws2, xs, xn, acc0, acc1, acc2, e_src, e_all, local, qd, own_st, own_de,
-    t_out, t_in, rim_src, rim, acts, sq_src, sq_all, ow_buf, ow_oth, part,
+    t_out, t_in, rim_src, rim, acts, sq_src, sq_all, ow_buf, ow_oth, part, half_way,
     x_send, x_recv, xf_send, xd_send, xd_recv, w_send, w_recv, up_send, dn_send, e_send, e_recv,
     t_send, t_recv, g_send, g_recv, a_send, a_recv, af_send, ad_send, ad_recv, q_send, q_recv,
     ou_send, on_send, o_recv, od_send, od_recv, m_send, m_recv,
@@ -702,20 +702,30 @@
             def _():
                 to_down(c, slot(c, b, g), b, g).wait_recv()
 
-    def gemm(c, a, first=False):
-        k = pl.ds(pl.multiple_of(a * n_fs * wr, n_fs * wr), n_fs * wr)
-        acc, w = accs[c], wss[c]
-
-        def each(i, _):
-            out = jnp.dot(xn[i, :, k], w[k, :], preferred_element_type=F32)
-            acc[i] = out if first else acc[i] + out
+    blk = n_fs * wr
+    total_k = n_sp * blk
+    is_end = jnp.logical_not(has_up & has_down)
+    near = pl.ds(pl.multiple_of(jnp.where(has_down, blk, 0), blk), total_k - blk)
+    far = pl.ds(pl.multiple_of(jnp.where(has_down, 0, total_k - blk), blk), blk)
+
+    def gemm(c, p, k, more):
+        out = jnp.dot(xn[p, :, k], wss[c][k, :], preferred_element_type=F32)
+        accs[c][p] = accs[c][p] + out if more else out
+
+    def main(c, p):
+        pl.when(is_end)(lambda: gemm(c, p, near, False))
+        pl.when(jnp.logical_not(is_end))(lambda: gemm(c, p, slice(0, total_k), False))
+
+    def each_pair(step):
+        def one(p, _):
+            step(p)
             return 0
 
-        lax.fori_loop(0, n_fs, each, 0)
-
-    def gemm_at(c, d):
-        pl.when(s - d >= 0)(lambda: gemm(c, s - d))
-        pl.when(s + d < n_sp)(lambda: gemm(c, s + d))
+        lax.fori_loop(0, 2, one, 0)
+
+    def last(c):
+        arrive(c, n_sp - 1)
+        pl.when(is_end)(lambda: each_pair(lambda p: gemm(c, p, far, True)))
 
     def x_slot(g, h, c):
         return xs.at[g, h * cut : (h + 1) * cut, cols(c)]
@@ -728,17 +738,19 @@
     def hand_on(g, h, here):
         send(rcopy(here, here, xd_send.at[g, h], xd_recv.at[g, h], other))
 
-    def norm(g):
+    def norm(j):
+        g = order[j]
         for h in range(2):
             here = x_slot(g, h, 1 - t)
             rcopy(here, here, xd_send.at[g, h], xd_recv.at[g, h], other).wait_recv()
         tile = 16
 
-        def each(j, _):
-            at = pl.ds(pl.multiple_of(j * tile, tile), tile)
+        def each(i, _):
+            at = pl.ds(pl.multiple_of(i * tile, tile), tile)
             feats = xs[g, at, :].astype(F32)
             scale = lax.rsqrt(jnp.mean(feats * feats, axis=-1, keepdims=True) + EPS)
-            xn[g, at, :] = (feats * scale * gain[...]).astype(BF)
+            to = pl.ds(pl.multiple_of((j % 2) * rows + i * tile, tile), tile)
+            xn[j // 2, to, :] = (feats * scale * gain[...]).astype(BF)
             return 0
 
         lax.fori_loop(0, rows // tile, each, 0, unroll=2)
@@ -812,36 +824,39 @@
         at = slice(i * gd, (i + 1) * gd)
         scaled = (gmap[t * (width // gd) + i].astype(F32) * pgain[:, at]).astype(BF)
         ow_buf[s, 1, at, :] = jnp.dot(scaled, wop[at, :], preferred_element_type=F32).astype(BF)
-    norm(f)
+    norm(0)
     relay(0, 1, order[:2])
     for i, (g, h, onto) in enumerate(((px, 0, py), (py, 1, px))):
         here = landed(g, h)
         send(rcopy(here, here, xf_send.at[i], x_recv.at[g, h], (s, onto, t)))
         hand_on(g, h, here)
     relay(0, 1, order[2:])
+    for d in range(2, n_sp - 1):
+        relay(0, d, order[:2])
     for g, h in ((px, 1), (py, 0)):
         hand_on(g, h, landed(g, h))
-    for d in range(2, n_sp - 1):
-        relay(0, d, order[:2])
-    norm(px)
-    norm(py)
+    norm(1)
     for d in range(2, n_sp - 1):
         relay(0, d, order[2:])
     both(1, src1.at[f], s, f)
     for g in order[1:]:
         from_square(1, g)
+    norm(2)
+    for d in range(1, n_sp - 1):
+        arrive(0, d)
+    main(0, 0)
+    relay(1, 1, order)
     for h in range(2):
         hand_on(pd, h, landed(pd, h))
-    norm(pd)
-
-    for d in range(1, n_sp - 1):
-        arrive(0, d)
-    gemm(0, s, True)
-    for d in range(1, n_sp - 1):
-        gemm_at(0, d)
-    relay(1, 1, order)
-    arrive(0, n_sp - 1)
-    gemm_at(0, n_sp - 1)
+    for d in range(2, n_sp - 1):
+        relay(1, d, order)
+    both(2, src2.at[f], s, f)
+    for g in order[1:]:
+        from_square(2, g)
+    norm(3)
+    main(0, 1)
+    relay(2, 1, order)
+    last(0)
     for g in order[1:]:
         rcopy(e_src.at[f], e_all.at[g], e_send.at[0], e_recv.at[g], other).wait_recv()
 
@@ -853,15 +868,17 @@
     lower = jnp.where(causal, 1.0, 0.0).astype(BF)
     lower = jnp.concatenate([lower, lower], axis=1)
 
-    def scan(g):
+    def scan(j):
+        p, base = j // 2, j % 2 * rows
         state = None
         so_far = jnp.zeros((1, ch), F32)
-        e_cols = e_all[g].T
+        e_cols = e_all[order[j]].T
         for n in range(rows // size):
             here = slice(n * size, (n + 1) * size)
-            v = acc0[g, here, 2 * ch : 3 * ch].astype(BF)
-            q = jax.nn.silu(acc0[g, here, 0:ch].astype(BF).astype(F32))
-            k = gap_f * jax.nn.sigmoid(-acc0[g, here, ch : 2 * ch].astype(BF).astype(F32))
+            there = slice(base + n * size, base + (n + 1) * size)
+            v = acc0[p, there, 2 * ch : 3 * ch].astype(BF)
+            q = jax.nn.silu(acc0[p, there, 0:ch].astype(BF).astype(F32))
+            k = gap_f * jax.nn.sigmoid(-acc0[p, there, ch : 2 * ch].astype(BF).astype(F32))
             logs = jnp.log1p(-k) + e_cols[here, 0:1]
             high = logs.astype(BF)
             low = (logs - high.astype(F32)).astype(BF)
@@ -875,21 +892,16 @@
             out = mm(scores, v, NN)
             if n:
                 out = out + mm(q_up, (state * jnp.exp(mid)).astype(BF), NT)
-            local[g, here, :] = out
-            qd[g, here, :] = (q * jnp.exp(mid + so_far)).astype(BF)
+            local[j, here, :] = out
+            qd[j, here, :] = (q * jnp.exp(mid + so_far)).astype(BF)
             fresh = mm(v, k, TN) * jnp.exp(end - mid)
             state = state * jnp.exp(end) + fresh if n else fresh
             so_far = so_far + end
-        own_st[g] = state
-        own_de[g] = jnp.broadcast_to(jnp.exp(so_far), own_de.shape[1:])
+        own_st[j] = state
+        own_de[j] = jnp.broadcast_to(jnp.exp(so_far), own_de.shape[1:])
 
     scan(0)
     scan(1)
-    for d in range(2, n_sp - 1):
-        relay(1, d, order)
-    both(2, src2.at[f], s, f)
-    for g in order[1:]:
-        from_square(2, g)
     scan(2)
     scan(3)
 
@@ -904,23 +916,19 @@
         for g in range(n_fs):
             carry(g).start()
 
+    for d in range(2, n_sp - 1):
+        relay(2, d, order)
     for d in range(1, n_sp - 1):
-        relay(2, d, order)
-
-    def project(c):
-        gemm(c, s, True)
-        for d in range(1, n_sp - 1):
-            arrive(c, d)
-            gemm_at(c, d)
-        arrive(c, n_sp - 1)
-        gemm_at(c, n_sp - 1)
-
-    project(1)
+        arrive(1, d)
+    each_pair(lambda p: main(1, p))
+    last(1)
     reach = rim.shape[1]
-    rim_src[...] = acc1[:, rows - reach :, :].astype(BF)
+    for j in range(n_fs):
+        rim_src[j] = acc1[j // 2, (j % 2 + 1) * rows - reach : (j % 2 + 1) * rows, :].astype(BF)
     edge = rcopy(rim_src, rim, g_send, g_recv, up)
     when(has_up, edge)
 
+    pl.when(jnp.logical_not(is_end))(lambda: each_pair(lambda p: main(2, p)))
     @pl.when(has_down & has_up)
     def _():
         for g in range(n_fs):
@@ -942,21 +950,24 @@
         window = jnp.where(group == level, 2 ** (level + 1), window)
     share = 1.0 / jnp.minimum(spot + 1, window).astype(F32)
 
-    def pool(g):
-        zp = acc1[g].astype(BF).astype(F32)
-        running = jnp.concatenate([rim[g].astype(F32), zp], axis=0)
+    def rows_of(g):
+        return pl.ds(pl.multiple_of(g * rows, rows), rows)
+
+    def pool(j):
+        zp = acc1[j // 2, j % 2 * rows : (j % 2 + 1) * rows, :].astype(BF).astype(F32)
+        running = jnp.concatenate([rim[j].astype(F32), zp], axis=0)
         total = None
         for level in range(POOL_GROUPS):
             stride = 2**level
             running = running[stride:] + running[:-stride]
             now = running[running.shape[0] - rows :]
             total = now if level == 0 else jnp.where(group == level, now, total)
-        acts[1, t, f, g * rows : (g + 1) * rows, :] = (total * share - zp).astype(BF)
+        acts[1, t, f, rows_of(order[j]), :] = (total * share - zp).astype(BF)
 
     part_rows = n_fs * rows // 2
 
     def a_slot(k, u, g, h):
-        return acts.at[k, u, g, h * part_rows : (h + 1) * part_rows, :]
+        return acts.at[k, u, g, pl.ds(pl.multiple_of(h * part_rows, part_rows), part_rows), :]
 
     def publish(k, h):
         here = a_slot(k, t, f, h)
@@ -988,21 +999,16 @@
                 here = a_slot(k, 1 - t, g, h)
                 rcopy(here, here, ad_send.at[k, g, h], ad_recv.at[k, g, h], other).wait_recv()
 
-    for h in range(2):
-        for g in range(h * n_fs // 2, (h + 1) * n_fs // 2):
-            pool(g)
+    halves = (f // 2, 1 - f // 2)
+    for i, h in enumerate(halves):
+        pool(2 * i)
+        pool(2 * i + 1)
         publish(1, h)
-    ow_relay(1, 1)
-    for d in range(2, n_sp - 1):
-        ow_relay(d, 0)
-    gemm(2, s, True)
     for d in range(1, n_sp - 1):
         arrive(2, d)
-        gemm_at(2, d)
+    pl.when(is_end)(lambda: each_pair(lambda p: gemm(2, p, near, False)))
     a_forward(1)
-    arrive(2, n_sp - 1)
-    gemm_at(2, n_sp - 1)
-
+    last(2)
     @pl.when(has_down & jnp.logical_not(has_up))
     def _():
         for g in range(n_fs):
@@ -1010,33 +1016,37 @@
 
     ones = jnp.ones((8, ch), BF)
 
-    def finish(g):
-        rec = local[g] + mm(qd[g], t_in[g], NT)
+    def finish(j):
+        g = order[j]
+        rec = local[j] + mm(qd[j], t_in[j], NT)
         sums = mm(ones, (rec * rec).astype(BF), NT)
         for i in range(lanes):
-            sq_src[g * lanes + i : g * lanes + i + 1, :] = sums[0:1, i * 128 : (i + 1) * 128]
-        gate = jax.nn.silu(acc2[g].astype(BF).astype(F32))
-        acts[0, t, f, g * rows : (g + 1) * rows, :] = (rec * gain_f * gate).astype(BF)
-
-    for h in range(2):
-        for g in range(h * n_fs // 2, (h + 1) * n_fs // 2):
-            finish(g)
+            sq_src[pl.ds(g * lanes + i, 1), :] = sums[0:1, i * 128 : (i + 1) * 128]
+        gate = jax.nn.silu(acc2[j // 2, j % 2 * rows : (j % 2 + 1) * rows, :].astype(BF).astype(F32))
+        acts[0, t, f, rows_of(g), :] = (rec * gain_f * gate).astype(BF)
+
+    for i, h in enumerate(halves):
+        finish(2 * i)
+        finish(2 * i + 1)
         publish(0, h)
     for i, g in enumerate(order[1:]):
         for u in range(n_tp):
             send(rcopy(sq_src, sq_all.at[t, f], q_send.at[i, u], q_recv.at[t, f], (s, g, u)))
     send(rcopy(sq_src, sq_all.at[t, f], q_send.at[n_fs - 1, 0], q_recv.at[t, f], other))
     sq_all[t, f] = sq_src[...]
+    ow_relay(1, 1)
+    a_rest(1)
+    for d in range(2, n_sp - 1):
+        ow_relay(d, 0)
+    a_forward(0)
     for d in range(2, n_sp - 1):
         ow_relay(d, 1)
-    a_rest(1)
     for k in range(2):
         ow_take(1, k)
-    a_forward(0)
+    a_rest(0)
     for d in range(2, n_sp - 1):
         for k in range(2):
             ow_take(d, k)
-    a_rest(0)
     a_other(1)
     a_other(0)
     for g in order[1:]:
@@ -1060,28 +1070,30 @@
             part.at[i, g, u], final.at[:, spot_of(t * n_half + i, f)], m_send.at[i, g, u], m_recv.at[i, f, t], (s, g, u)
         )
 
+    def weight_side(k, a, i, g):
+        here = pl.ds(g * rows, rows)
+        total = None
+        for u, w in ((t, ow_buf.at[a, k]), (1 - t, ow_oth.at[i, k])):
+            left = jnp.concatenate([acts[k, u, b, here, :] for b in range(n_fs)], axis=1)
+            now = jnp.dot(left, w[...], preferred_element_type=F32)
+            total = now if total is None else total + now
+        return total
+
     for j in range(n_half):
         i = jnp.where(late, n_half - 1 - j, j)
         a = t * n_half + i
-        if j == n_half - 1:
-            for k in range(2):
+        for k in range(2):
+            if j == n_half - 1:
                 ow_take(n_sp - 1, k)
-        for k in range(2):
             rcopy(ow_buf.at[a, k], ow_oth.at[i, k], od_send.at[a, k], od_recv.at[i, k], other).wait_recv()
-        for g in range(n_fs):
-            here = pl.ds(g * rows, rows)
-            made = []
-            for k in range(2):
-                total = None
-                for u, w in ((t, ow_buf.at[a, k]), (1 - t, ow_oth.at[i, k])):
-                    left = jnp.concatenate([acts[k, u, b, here, :] for b in range(n_fs)], axis=1)
-                    now = jnp.dot(left, w[...], preferred_element_type=F32)
-                    total = now if total is None else total + now
-                made.append(total)
-            mixed = (made[0] * scales[g] + made[1]).astype(BF)
-            for u in range(n_tp):
-                part[i, g, u] = mixed[u * out_rows : (u + 1) * out_rows]
-                when((g != f) | (u != t), piece(i, g, u))
+            for g in range(n_fs):
+                if k == 0:
+                    half_way[g] = weight_side(0, a, i, g) * scales[g]
+                    continue
+                mixed = (half_way[g] + weight_side(1, a, i, g)).astype(BF)
+                for u in range(n_tp):
+                    part[i, g, u] = mixed[u * out_rows : (u + 1) * out_rows]
+                    when((g != f) | (u != t), piece(i, g, u))
         final[:, spot_of(a, f)] = part[i, f, t]
 
     for i in range(n_half):
@@ -1149,8 +1161,8 @@
         [
             buf(BF, n_fs, wr, 3 * ch), buf(BF, n_fs, wr, ch), buf(BF, n_fs, wr, ch),
             buf(BF, feats, 3 * ch), buf(BF, feats, ch), buf(BF, feats, ch),
-            buf(BF, n_fs, rows, n_tp * half), buf(BF, n_fs, rows, n_tp * half),
-            buf(F32, n_fs, rows, 3 * ch), buf(F32, n_fs, rows, ch), buf(F32, n_fs, rows, ch),
+            buf(BF, n_fs, rows, n_tp * half), buf(BF, 2, n_fs // 2 * rows, n_tp * half),
+            buf(F32, 2, n_fs // 2 * rows, 3 * ch), buf(F32, 2, n_fs // 2 * rows, ch), buf(F32, 2, n_fs // 2 * rows, ch),
             buf(F32, n_fs, 8, rows), buf(F32, n_fs, 8, rows),
             buf(F32, n_fs, rows, ch), buf(BF, n_fs, rows, ch),
             buf(F32, n_fs, ch, ch), buf(F32, n_fs, 8, ch),
@@ -1159,7 +1171,7 @@
             buf(BF, 2, n_tp, n_fs, n_fs * rows, ch),
             buf(F32, n_fs * lanes, 128), buf(F32, n_tp, n_fs, n_fs * lanes, 128),
             buf(BF, n_sp, 2, width, cw), buf(BF, n_half, 2, width, cw),
-            buf(BF, n_half, n_fs, n_tp, rows // n_tp, cw),
+            buf(BF, n_half, n_fs, n_tp, rows // n_tp, cw), buf(F32, n_fs, rows, cw),
             dma(2, 2), dma(n_fs, 2), dma(2), dma(n_fs, 2), dma(n_fs, 2),
             dma(3, n_fs - 1), dma(3, n_sp, n_fs), dma(3, n_sp, n_fs), dma(3, n_sp, n_fs), dma(n_fs - 1), dma(n_fs),
             dma(n_fs), dma(n_fs), dma(), dma(),

time: 98.5 us -> 89.1 us (0.905)
  the two profiles are of different devices: /device:TPU:23 before, /device:TPU:29 now
where the time goes in v2:
time: 89.1 us; the launch traced here: 88.6 us
  Pallas kernels  85.2 us (96%)
  local copies, waits for them, and re-layouts  3.37 us (4%)
    pallas_call x1, Pallas kernels, fused(): comm(functools.partial(layer_kernel, n_sp, n_fs, n_tp), [((rows // n_tp,...  85.2 us
    unnamed x4, local copies, waits for them, and re-layouts  3.37 us

profile of v2, /device:TPU:29, one launch (start us, length us, event | category | flops | bytes accessed | tf_op | source)
XLA Modules:
  0.0 88.6 jit_solution(14271419151606005057)
XLA Ops:
  0.0 0.0 copy-start
  0.0 0.7 copy-done
  0.7 0.8 copy.15
  1.5 85.2 %layer.1 = bf16[128,2048]{1,0:T(8,128)(2,1)} custom-call(bf16[256,1024]{1,0:T(8,128)(2,1)} %bitcast.9, bf16[128,512]{1,0:T(8,128)(2,1)} %wq.1, bf16[128,512]{1,0:T(8,128)(2,1)} %wf.1, bf16[128,512]{1,0:T(8,128)(2,1)} %wi.1, bf16[128,512]{1,0:T(8,128)(2,1)} %wo.1, bf16[128,512]{1,0:T(8,128)(2,1)} %wp.1, f32[256,4]{1,0:T(8,128)} %bitcast.8, ...), custom_call_target="tpu_custom_call" | custom-call | tf_op jit(solution)/shard_map/layer/pallas_call | solution.py:1158
  86.7 1.9 %copy.17 = bf16[1,128,2048]{2,1,0:T(8,128)(2,1)} copy(bf16[1,128,2048]{2,1,0:T(8,128)(2,1)} %bitcast.7) | data formatting | bytes 1048576
Async XLA Ops:
  0.0 0.7 copy-start

commit v3 on v0

--- a/solution.py
+++ b/solution.py
@@ -521,11 +521,12 @@
     return pltpu.SemaphoreType.DMA(shape) if shape else pltpu.SemaphoreType.DMA
 
 
-def comm(kernel, outs, scratch, number, name):
+def comm(kernel, outs, scratch, number, name, ins=None):
     return pl.pallas_call(
         kernel,
         out_shape=[jax.ShapeDtypeStruct(a, b) for a, b in outs],
         out_specs=vmem(len(outs)),
+        **({} if ins is None else {"in_specs": ins}),
         scratch_shapes=scratch,
         compiler_params=pltpu.CompilerParams(
             collective_id=number, has_side_effects=True, vmem_limit_bytes=60 * 1024 * 1024
@@ -590,6 +591,664 @@
     return final[None]
 
 
+def mm(a, b, dims):
+    return lax.dot_general(a, b, (dims, ((), ())), preferred_element_type=F32)
+
+
+NN, NT, TN = ((1,), (0,)), ((1,), (1,)), ((0,), (0,))
+
+
+def layer_kernel(
+    n_sp, n_fs, n_tp, tok, wq, wf, wi, wo, wp, extra_in, gain_in, gap_in, rec_gain_in, gmap_in, pgain_in, wor, wop_in, final,
+    src0, src1, src2, ws0, ws1, ws2, xs, xn, acc0, acc1, acc2, e_src, e_all, local, qd, own_st, own_de,
+    t_out, t_in, rim_src, rim, acts, sq_src, sq_all, ow_buf, ow_oth, part, half_way,
+    extra, gain, gap, rec_gain, gmap, pgain, wop,
+    in_sem, w_in, p_in, x_send, x_recv, xd_send, xd_recv, w_send, w_recv, b_recv, ba_recv, up_send, dn_send, e_send, e_recv,
+    t_send, t_recv, g_send, g_recv, a_send, a_recv, ad_send, ad_recv, q_send, q_recv,
+    ou_send, on_send, o_recv, od_send, od_recv, m_send, m_recv,
+):
+    s, f, t = place()
+    rows, half = tok.shape
+    cut = rows // 2
+    wr, width = wq.shape
+    ch = width // n_fs
+    cw = wor.shape[1]
+    n_half = n_sp // n_tp
+    out_rows = rows // n_tp
+    lanes = rows // 128
+    size = 128
+    blk = n_fs * wr
+    total_k = n_sp * blk
+    groups = ((wq, wf, wi), (wp,), (wo,))
+    srcs, wss, accs = (src0, src1, src2), (ws0, ws1, ws2), (acc0, acc1, acc2)
+    other = (s, f, 1 - t)
+    px, py, pd = square(f)
+    order = (f, px, py, pd)
+    up, down = (s + 1, f, t), (s - 1, f, t)
+    has_up, has_down = s < n_sp - 1, s > 0
+    is_end = jnp.logical_not(has_up & has_down)
+
+    def when(cond, *copies):
+        @pl.when(cond)
+        def _():
+            for c in copies:
+                c.start()
+
+    def sent(ref, sem):
+        rcopy(ref, ref, sem, sem, other).wait_send()
+
+    def came(ref, sem):
+        rcopy(ref, ref, sem, sem, other).wait_recv()
+
+    def cols(c):
+        return pl.ds(pl.multiple_of(c * half, half), half)
+
+    def span(a, b):
+        return pl.ds(pl.multiple_of((a * n_fs + b) * wr, wr), wr)
+
+    def slot(c, a, b):
+        return wss[c].at[span(a, b), :]
+
+    def block(c, a):
+        return wss[c].at[pl.ds(pl.multiple_of(a * blk, blk), blk), :]
+
+    def x_slot(g, h, c):
+        return xs.at[g, h * cut : (h + 1) * cut, cols(c)]
+
+    peers = (
+        [(None, other)]
+        + [(None, (s, g, u)) for g in order[1:] for u in (t, 1 - t)]
+        + [(has_up, up), (has_down, down)]
+    )
+    barrier = pltpu.get_barrier_semaphore()
+    for cond, dev in peers:
+        def tell(dev=dev):
+            pl.semaphore_signal(barrier, inc=1, device_id=dev, device_id_type=MESH)
+        if cond is None:
+            tell()
+        else:
+            pl.when(cond)(tell)
+    for c in range(3):
+        for i, w in enumerate(groups[c]):
+            for j, g in enumerate(order):
+                lane = pl.ds(pl.multiple_of(g * ch, ch), ch)
+                into = wss[c].at[span(s, f), i * ch : (i + 1) * ch] if j == 0 else srcs[c].at[j - 1, :, i * ch : (i + 1) * ch]
+                pltpu.make_async_copy(w.at[:, lane], into, w_in.at[c, min(j, 1)]).start()
+        if c == 0:
+            pltpu.make_async_copy(tok, xs.at[f, :, cols(t)], in_sem.at[0]).start()
+            pltpu.make_async_copy(wor, ow_buf.at[s, 0], in_sem.at[1]).start()
+    params = ((extra_in, extra), (gain_in, gain), (gmap_in, gmap), (pgain_in, pgain), (wop_in, wop), (gap_in, gap), (rec_gain_in, rec_gain))
+    loads = [pltpu.make_async_copy(a, b, p_in.at[i]) for i, (a, b) in enumerate(params)]
+    for c in loads:
+        c.start()
+    pl.semaphore_wait(barrier, sum(1 if cond is None else jnp.where(cond, 1, 0) for cond, _ in peers))
+
+    def took(ref, sem):
+        pltpu.make_async_copy(ref, ref, sem).wait()
+
+    def to_up(src, b, a):
+        return rcopy(src, slot(0, a, b), up_send.at[0], w_recv.at[a, b], up)
+
+    def to_down(src, b, a):
+        return rcopy(src, slot(0, a, b), dn_send.at[0], w_recv.at[a, b], down)
+
+    def both(a, b):
+        when(has_up, to_up(slot(0, a, b), b, a))
+        when(has_down, to_down(slot(0, a, b), b, a))
+
+    def b_up(c, a):
+        return rcopy(block(c, a), block(c, a), up_send.at[c], b_recv.at[c - 1, a], up)
+
+    def b_down(c, a):
+        return rcopy(block(c, a), block(c, a), dn_send.at[c], b_recv.at[c - 1, a], down)
+
+    def spread(c):
+        for j, g in enumerate(order[1:]):
+            rsem = w_recv.at[s, f] if c == 0 else ba_recv.at[c - 1]
+            rcopy(srcs[c].at[j], slot(c, s, f), w_send.at[c], rsem, (s, g, t)).start()
+
+    def own_block(c):
+        came(wss[c].at[0 : (n_fs - 1) * wr, :], ba_recv.at[c - 1])
+        when(has_up, b_up(c, s))
+        when(has_down, b_down(c, s))
+
+    low = 2 * s < n_sp
+
+    def relay(c, d, gs=(None,)):
+        a, b = s - d, s + d
+
+        def rising(extra):
+            for g in gs:
+                @pl.when((a >= 0) & has_up & extra)
+                def _():
+                    hop = to_up(slot(0, a, g), g, a) if c == 0 else b_up(c, a)
+                    hop.wait_recv()
+                    hop.start()
+
+        def falling():
+            for g in gs:
+                @pl.when((b < n_sp) & has_down)
+                def _():
+                    hop = to_down(slot(0, b, g), g, b) if c == 0 else b_down(c, b)
+                    hop.wait_recv()
+                    hop.start()
+
+        rising(low)
+        falling()
+        rising(jnp.logical_not(low))
+
+    def arrive(c, d):
+        for g in order if c == 0 else (None,):
+            a, b = s - d, s + d
+
+            @pl.when((a >= 0) & jnp.logical_not(has_up))
+            def _():
+                (to_up(slot(0, a, g), g, a) if c == 0 else b_up(c, a)).wait_recv()
+
+            @pl.when((b < n_sp) & jnp.logical_not(has_down))
+            def _():
+                (to_down(slot(0, b, g), g, b) if c == 0 else b_down(c, b)).wait_recv()
+
+    near = pl.ds(pl.multiple_of(jnp.where(has_down, blk, 0), blk), total_k - blk)
+    far = pl.ds(pl.multiple_of(jnp.where(has_down, 0, total_k - blk), blk), blk)
+
+    def gemm(c, p, k, more):
+        out = jnp.dot(xn[p, :, k], wss[c][k, :], preferred_element_type=F32)
+        accs[c][p] = accs[c][p] + out if more else out
+
+    def main(c, p):
+        pl.when(is_end)(lambda: gemm(c, p, near, False))
+        pl.when(jnp.logical_not(is_end))(lambda: gemm(c, p, slice(0, total_k), False))
+
+    def each_pair(step):
+        def one(p, _):
+            step(p)
+            return 0
+
+        lax.fori_loop(0, 2, one, 0)
+
+    def last(c):
+        arrive(c, n_sp - 1)
+        pl.when(is_end)(lambda: each_pair(lambda p: gemm(c, p, far, True)))
+
+    def landed(g, h):
+        here = x_slot(g, h, t)
+        came(here, x_recv.at[g, h])
+        return here
+
+    def hand_on(g, h):
+        here = x_slot(g, h, t)
+        rcopy(here, here, xd_send, xd_recv.at[g], other).start()
+
+    def norm(j):
+        g = order[j]
+        came(xs.at[g, :, cols(1 - t)], xd_recv.at[g])
+        tile = 16
+
+        def each(i, _):
+            at = pl.ds(pl.multiple_of(i * tile, tile), tile)
+            feats = xs[g, at, :].astype(F32)
+            scale = lax.rsqrt(jnp.mean(feats * feats, axis=-1, keepdims=True) + EPS)
+            to = pl.ds(pl.multiple_of((j % 2) * rows + i * tile, tile), tile)
+            xn[j // 2, to, :] = (feats * scale * gain[...]).astype(BF)
+            return 0
+
+        lax.fori_loop(0, rows // tile, each, 0, unroll=2)
+
+    def ow_up(a, k):
+        return rcopy(ow_buf.at[a, k], ow_buf.at[a, k], ou_send, o_recv.at[a, k], up)
+
+    def ow_down(a, k):
+        return rcopy(ow_buf.at[a, k], ow_buf.at[a, k], on_send, o_recv.at[a, k], down)
+
+    def ow_share(a, k):
+        i = lax.rem(a, n_half)
+        when(a // n_half != t, rcopy(ow_buf.at[a, k], ow_oth.at[i, k], od_send, od_recv.at[i, k], other))
+
+    def ow_relay(d, k):
+        a, b = s - d, s + d
+
+        @pl.when((a >= 0) & has_up)
+        def _():
+            ow_up(a, k).wait_recv()
+            ow_up(a, k).start()
+            ow_share(a, k)
+
+        @pl.when((b < n_sp) & has_down)
+        def _():
+            ow_down(b, k).wait_recv()
+            ow_down(b, k).start()
+            ow_share(b, k)
+
+    def ow_take(d, k):
+        a, b = s - d, s + d
+
+        @pl.when((a >= 0) & jnp.logical_not(has_up))
+        def _():
+            ow_up(a, k).wait_recv()
+            ow_share(a, k)
+
+        @pl.when((b < n_sp) & jnp.logical_not(has_down))
+        def _():
+            ow_down(b, k).wait_recv()
+            ow_share(b, k)
+
+    took(slot(0, s, f), w_in.at[0, 0])
+    both(s, f)
+    took(srcs[0], w_in.at[0, 1])
+    spread(0)
+    took(xs.at[f, :, cols(t)], in_sem.at[0])
+    for p, hs in ((px, (0, 1)), (py, (1, 0))):
+        for h in hs:
+            rcopy(x_slot(f, h, t), x_slot(f, h, t), x_send, x_recv.at[f, h], (s, p, t)).start()
+    for h in range(2):
+        hand_on(f, h)
+    took(ow_buf.at[s, 0], in_sem.at[1])
+    when(has_up, ow_up(s, 0))
+    when(has_down, ow_down(s, 0))
+    for c in loads:
+        c.wait()
+    e_rows = extra[...].T
+    for g in range(n_fs):
+        e_src[g] = jnp.broadcast_to(e_rows[g : g + 1, :], e_src.shape[1:])
+    for g in order[1:]:
+        rcopy(e_src.at[g], e_all.at[f], e_send, e_recv, (s, g, t)).start()
+    for c in (1, 2):
+        took(slot(c, s, f), w_in.at[c, 0])
+        took(srcs[c], w_in.at[c, 1])
+        spread(c)
+    e_all[f] = e_src[f]
+    for g in order[1:]:
+        came(slot(0, s, g), w_recv.at[s, g])
+        both(s, g)
+    gd = gmap.shape[1]
+    for i in range(width // gd):
+        at = slice(i * gd, (i + 1) * gd)
+        scaled = (gmap[t * (width // gd) + i].astype(F32) * pgain[:, at]).astype(BF)
+        ow_buf[s, 1, at, :] = jnp.dot(scaled, wop[at, :], preferred_element_type=F32).astype(BF)
+    norm(0)
+    relay(0, 1, order[:2])
+    for g, h, onto in ((px, 0, py), (py, 1, px)):
+        here = landed(g, h)
+        rcopy(here, here, x_send, x_recv.at[g, h], (s, onto, t)).start()
+        hand_on(g, h)
+    relay(0, 1, order[2:])
+    for d in range(2, n_sp - 1):
+        relay(0, d, order[:2])
+    for g, h in ((px, 1), (py, 0)):
+        landed(g, h)
+        hand_on(g, h)
+    norm(1)
+    for d in range(2, n_sp - 1):
+        relay(0, d, order[2:])
+    own_block(1)
+    pl.when(is_end)(lambda: own_block(2))
+    norm(2)
+    for d in range(1, n_sp - 1):
+        arrive(0, d)
+    main(0, 0)
+    for h in range(2):
+        landed(pd, h)
+        hand_on(pd, h)
+    norm(3)
+    main(0, 1)
+    relay(1, 1)
+
+    reach = rim.shape[1]
+    edge = rcopy(rim_src, rim, g_send, g_recv, up)
+
+    def send_rim():
+        for j in range(n_fs):
+            rim_src[j] = acc1[j // 2, (j % 2 + 1) * rows - reach : (j % 2 + 1) * rows, :].astype(BF)
+        when(has_up, edge)
+
+    last(0)
+    came(e_all.at[0 : n_fs - 1], e_recv)
+
+    mine = pl.ds(pl.multiple_of(f * ch, ch), ch)
+    gap_f = gap[:, mine]
+    gain_f = rec_gain[:, mine]
+    at = lax.broadcasted_iota(jnp.int32, (size, size), 0)
+    causal = at >= lax.broadcasted_iota(jnp.int32, (size, size), 1)
+    lower = jnp.where(causal, 1.0, 0.0).astype(BF)
+    lower = jnp.concatenate([lower, lower], axis=1)
+
+    def scan(j):
+        p, base = j // 2, j % 2 * rows
+        state = None
+        so_far = jnp.zeros((1, ch), F32)
+        e_cols = e_all[order[j]].T
+        for n in range(rows // size):
+            here = slice(n * size, (n + 1) * size)
+            there = slice(base + n * size, base + (n + 1) * size)
+            v = acc0[p, there, 2 * ch : 3 * ch].astype(BF)
+            q = jax.nn.silu(acc0[p, there, 0:ch].astype(BF).astype(F32))
+            k = gap_f * jax.nn.sigmoid(-acc0[p, there, ch : 2 * ch].astype(BF).astype(F32))
+            logs = jnp.log1p(-k) + e_cols[here, 0:1]
+            high = logs.astype(BF)
+            low = (logs - high.astype(F32)).astype(BF)
+            within = mm(lower, jnp.concatenate([high, low], axis=0), NN)
+            mid = within[size // 2 - 1 : size // 2]
+            end = within[size - 1 :]
+            q = q * jnp.exp(within - mid)
+            k = (k * jnp.exp(mid - within)).astype(BF)
+            q_up = q.astype(BF)
+            scores = jnp.where(causal, mm(q_up, k, NT), 0.0).astype(BF)
+            out = mm(scores, v, NN)
+            if n:
+                out = out + mm(q_up, (state * jnp.exp(mid)).astype(BF), NT)
+            local[j, here, :] = out
+            qd[j, here, :] = (q * jnp.exp(mid + so_far)).astype(BF)
+            fresh = mm(v, k, TN) * jnp.exp(end - mid)
+            state = state * jnp.exp(end) + fresh if n else fresh
+            so_far = so_far + end
+        own_st[j] = state
+        own_de[j] = jnp.broadcast_to(jnp.exp(so_far), own_de.shape[1:])
+
+    def carry(g):
+        return rcopy(t_out.at[g], t_in.at[g], t_send, t_recv.at[g], up)
+
+    for j in range(n_fs):
+        scan(j)
+
+        @pl.when(jnp.logical_not(has_down))
+        def _():
+            t_in[j] = jnp.zeros(t_in.shape[1:], BF)
+            t_out[j] = own_st[j].astype(BF)
+            carry(j).start()
+
+    for d in range(2, n_sp - 1):
+        relay(1, d)
+    pl.when(jnp.logical_not(is_end))(lambda: own_block(2))
+    @pl.when(jnp.logical_not(is_end))
+    def _():
+        each_pair(lambda p: gemm(1, p, slice(0, total_k), False))
+        send_rim()
+
+    relay(2, 1)
+    def chain():
+        for g in range(n_fs):
+            carry(g).wait_recv()
+            t_out[g] = (own_st[g] + t_in[g].astype(F32) * own_de[g, 0:1, :]).astype(BF)
+            carry(g).start()
+
+    group = (t * n_fs * ch + f * ch) // gd
+    spot = s * rows + lax.broadcasted_iota(jnp.int32, (rows, ch), 0)
+    window = 2
+    for level in range(1, POOL_GROUPS):
+        window = jnp.where(group == level, 2 ** (level + 1), window)
+    share = 1.0 / jnp.minimum(spot + 1, window).astype(F32)
+
+    def rows_of(g):
+        return pl.ds(pl.multiple_of(g * rows, rows), rows)
+
+    def pool(j):
+        zp = acc1[j // 2, j % 2 * rows : (j % 2 + 1) * rows, :].astype(BF).astype(F32)
+        running = jnp.concatenate([rim[j].astype(F32), zp], axis=0)
+        total = None
+        for level in range(POOL_GROUPS):
+            stride = 2**level
+            running = running[stride:] + running[:-stride]
+            now = running[running.shape[0] - rows :]
+            total = now if level == 0 else jnp.where(group == level, now, total)
+        acts[1, t, f, rows_of(order[j]), :] = (total * share - zp).astype(BF)
+
+    part_rows = n_fs * rows // 2
+    quarter = part_rows // 2
+
+    def a_slot(k, u, g, h, q=None):
+        lo, n = (h * part_rows, part_rows) if q is None else (h * part_rows + q * quarter, quarter)
+        return acts.at[k, u, g, lo : lo + n, :]
+
+    def a_share(k, g, h):
+        here = a_slot(k, t, g, h)
+        rcopy(here, here, ad_send, ad_recv.at[k, h], other).start()
+
+    def publish(k):
+        for h in range(2):
+            here = a_slot(k, t, f, h)
+            for p in (px, py):
+                rcopy(here, here, a_send, a_recv.at[k, f, h], (s, p, t)).start()
+            a_share(k, f, h)
+
+    def a_forward(k, h):
+        for g, q, onto in ((px, 0, py), (py, 1, px)):
+            came(a_slot(k, t, g, h), a_recv.at[k, g, h])
+            here = a_slot(k, t, g, h, q)
+            rcopy(here, here, a_send, a_recv.at[k, g, h], (s, onto, t)).start()
+            a_share(k, g, h)
+
+    def a_rest(k, h):
+        came(a_slot(k, t, pd, h), a_recv.at[k, pd, h])
+        a_share(k, pd, h)
+
+    def a_other(k, h):
+        came(acts.at[k, 1 - t, :, h * part_rows : (h + 1) * part_rows, :], ad_recv.at[k, h])
+
+    def pool_all():
+        pl.when(has_down)(edge.wait_recv)
+        for j in range(n_fs):
+            pool(j)
+        publish(1)
+
+    mid_low = jnp.logical_not(is_end) & low
+    mid_high = jnp.logical_not(is_end) & jnp.logical_not(low)
+    pl.when(mid_low)(chain)
+    for d in range(2, n_sp - 1):
+        relay(2, d)
+    pl.when(jnp.logical_not(is_end))(lambda: each_pair(lambda p: gemm(2, p, slice(0, total_k), False)))
+    pl.when(mid_high)(pool_all)
+    pl.when(mid_high)(chain)
+    when(has_up, ow_up(s, 1))
+    when(has_down, ow_down(s, 1))
+    for k in range(2):
+        ow_share(s, k)
+    ow_relay(1, 0)
+    for d in range(1, n_sp - 1):
+        arrive(1, d)
+    pl.when(is_end)(lambda: each_pair(lambda p: gemm(1, p, near, False)))
+    last(1)
+    @pl.when(is_end)
+    def _():
+        send_rim()
+
+        @pl.when(jnp.logical_not(has_down))
+        def _():
+            rim[...] = jnp.zeros(rim.shape, BF)
+
+    pl.when(jnp.logical_not(mid_high))(pool_all)
+    ones = jnp.ones((8, ch), BF)
+
+    def finish(j):
+        g = order[j]
+        rec = local[j] + mm(qd[j], t_in[j], NT)
+        sums = mm(ones, (rec * rec).astype(BF), NT)
+        for i in range(lanes):
+            sq_src[pl.ds(g * lanes + i, 1), :] = sums[0:1, i * 128 : (i + 1) * 128]
+        gate = jax.nn.silu(acc2[j // 2, j % 2 * rows : (j % 2 + 1) * rows, :].astype(BF).astype(F32))
+        acts[0, t, f, rows_of(g), :] = (rec * gain_f * gate).astype(BF)
+
+    def finish_all():
+        for j in range(n_fs):
+            finish(j)
+        for u, g in [(1 - t, f)] + [(u, g) for g in order[1:] for u in (t, 1 - t)]:
+            rcopy(sq_src, sq_all.at[t * n_fs + f], q_send, q_recv, (s, g, u)).start()
+        publish(0)
+        sq_all[t * n_fs + f] = sq_src[...]
+
+    pl.when(jnp.logical_not(is_end))(finish_all)
+    for d in range(1, n_sp - 1):
+        arrive(2, d)
+    pl.when(is_end)(lambda: each_pair(lambda p: gemm(2, p, near, False)))
+    a_forward(1, 0)
+    ow_relay(1, 1)
+    a_forward(1, 1)
+    last(2)
+    @pl.when(has_down & jnp.logical_not(has_up))
+    def _():
+        for g in range(n_fs):
+            carry(g).wait_recv()
+
+    pl.when(is_end)(finish_all)
+    for d in range(2, n_sp - 1):
+        ow_relay(d, 0)
+    for h in range(2):
+        a_rest(1, h)
+    for d in range(2, n_sp - 1):
+        ow_relay(d, 1)
+    a_forward(0, 0)
+    a_forward(0, 1)
+    for d in range(1, n_sp - 1):
+        for k in range(2):
+            ow_take(d, k)
+    came(sq_all.at[0 : n_tp * n_fs - 1], q_recv)
+    sums = sum(sq_all[i] for i in range(n_tp * n_fs))
+    scale = lax.rsqrt(sums / (n_tp * width) + EPS).T
+    half_lanes = n_fs * lanes // 2
+    scales = [
+        jnp.concatenate([scale[:, h * half_lanes + i : h * half_lanes + i + 1] for i in range(half_lanes)], axis=0)
+        for h in range(2)
+    ]
+    late = s - t * n_half >= n_half - 1
+
+    def spot_of(a, g):
+        return pl.ds(pl.multiple_of((a * n_fs + g) * cw, cw), cw)
+
+    def at_part(i, g, u):
+        return (i * n_fs + g) * n_tp + u
+
+    def piece(i, g, u):
+        return rcopy(part.at[at_part(i, g, u)], final.at[:, spot_of(t * n_half + i, f)], m_send, m_recv, (s, g, u))
+
+    def weight_side(k, a, i, h):
+        here = slice(h * part_rows, (h + 1) * part_rows)
+        total = None
+        for u, w in ((t, ow_buf.at[a, k]), (1 - t, ow_oth.at[i, k])):
+            left = jnp.concatenate([acts[k, u, b, here, :] for b in range(n_fs)], axis=1)
+            now = jnp.dot(left, w[...], preferred_element_type=F32)
+            total = now if total is None else total + now
+        return total
+
+    def rec_side(a, i, h):
+        half_way[h] = weight_side(0, a, i, h) * scales[h]
+
+    def pool_side(a, i, h):
+        mixed = (half_way[h] + weight_side(1, a, i, h)).astype(BF)
+        for g in range(h * n_fs // 2, (h + 1) * n_fs // 2):
+            for u in range(n_tp):
+                lo = (g * n_tp + u) * out_rows - h * part_rows
+                part[at_part(i, g, u)] = mixed[lo : lo + out_rows]
+                when((g != f) | (u != t), piece(i, g, u))
+
+    def ow_got(j, k):
+        i = jnp.where(late, n_half - 1 - j, j)
+        if j == n_half - 1:
+            ow_take(n_sp - 1, k)
+        came(ow_oth.at[i, k], od_recv.at[i, k])
+        return t * n_half + i, i
+
+    for j in range(n_half):
+        if j == 0:
+            for k in range(2):
+                a, i = ow_got(0, k)
+            for h in range(2):
+                a_rest(0, h)
+                for k in range(2):
+                    a_other(k, h)
+                rec_side(a, i, h)
+                pool_side(a, i, h)
+        else:
+            a, i = ow_got(j, 0)
+            for h in range(2):
+                rec_side(a, i, h)
+            a, i = ow_got(j, 1)
+            for h in range(2):
+                pool_side(a, i, h)
+        final[:, spot_of(a, f)] = part[at_part(i, f, t)]
+
+    pieces = part.at[0 : n_half * (n_tp * n_fs - 1)]
+    came(pieces, m_recv)
+    sent(pieces, m_send)
+    sent(xs.at[0:3, :, 0:half], x_send)
+    sent(xs.at[:, :, 0:half], xd_send)
+    sent(e_src.at[0 : n_fs - 1], e_send)
+    for c in range(3):
+        sent(srcs[c], w_send.at[c])
+    sent(acts.at[:, 0, 0:3], a_send)
+    sent(acts.at[:, 0], ad_send)
+    sent(sq_all.at[0 : n_tp * n_fs - 1], q_send)
+    sent(ow_oth, od_send)
+    for v in range(n_sp):
+        @pl.when(s == v)
+        def _():
+            if v < n_sp - 1:
+                for c in range(3):
+                    sent(wss[c].at[0 : (v + 1) * blk, :], up_send.at[c])
+                sent(ow_buf.at[0 : v + 1], ou_send)
+                sent(rim_src, g_send)
+                sent(t_out, t_send)
+            if v > 0:
+                for c in range(3):
+                    sent(wss[c].at[0 : (n_sp - v) * blk, :], dn_send.at[c])
+                sent(ow_buf.at[0 : n_sp - v], on_send)
+
+
+def fused(
+    n_sp, n_fs, n_tp, tokens, norm_gain, w_query, forget_weight, w_input, w_outgate, w_pool, forget_gap,
+    extra_decay, rec_gain, group_weight, pool_gain, recurrent_output_weight, w_out_pool,
+):
+    rows, half = tokens.shape[1:]
+    wr, width = w_query.shape
+    ch = width // n_fs
+    cw = w_out_pool.shape[1]
+    n_half = n_sp // n_tp
+    feats = n_sp * n_fs * wr
+    lanes = rows // 128
+
+    def buf(kind, *shape):
+        return pltpu.VMEM(shape, kind)
+
+    args = (
+        tokens[0], w_query, forget_weight, w_input, w_outgate, w_pool, extra_decay[0], norm_gain[None],
+        forget_gap[None], rec_gain[None], group_weight, pool_gain[None], recurrent_output_weight, w_out_pool,
+    )
+    extra, gain, gap, r_gain, gmap, pgain = args[6:12]
+    (final,) = comm(
+        functools.partial(layer_kernel, n_sp, n_fs, n_tp),
+        [((rows // n_tp, n_sp * n_fs * cw), BF)],
+        [
+            buf(BF, n_fs - 1, wr, 3 * ch), buf(BF, n_fs - 1, wr, ch), buf(BF, n_fs - 1, wr, ch),
+            buf(BF, feats, 3 * ch), buf(BF, feats, ch), buf(BF, feats, ch),
+            buf(BF, n_fs, rows, n_tp * half), buf(BF, 2, n_fs // 2 * rows, n_tp * half),
+            buf(F32, 2, n_fs // 2 * rows, 3 * ch), buf(F32, 2, n_fs // 2 * rows, ch), buf(F32, 2, n_fs // 2 * rows, ch),
+            buf(F32, n_fs, 8, rows), buf(F32, n_fs, 8, rows),
+            buf(F32, n_fs, rows, ch), buf(BF, n_fs, rows, ch),
+            buf(F32, n_fs, ch, ch), buf(F32, n_fs, 8, ch),
+            buf(BF, n_fs, ch, ch), buf(BF, n_fs, ch, ch),
+            buf(BF, n_fs, 2**POOL_GROUPS, ch), buf(BF, n_fs, 2**POOL_GROUPS, ch),
+            buf(BF, 2, n_tp, n_fs, n_fs * rows, ch),
+            buf(F32, n_fs * lanes, 128), buf(F32, n_tp * n_fs, n_fs * lanes, 128),
+            buf(BF, n_sp, 2, width, cw), buf(BF, n_half, 2, width, cw),
+            buf(BF, n_half * n_fs * n_tp, rows // n_tp, cw), buf(F32, 2, n_fs // 2 * rows, cw),
+        ]
+        + [buf(a.dtype, *a.shape) for a in (extra, gain, gap, r_gain, gmap, pgain, w_out_pool)]
+        + [
+            dma(2), dma(3, 2), dma(7), dma(), dma(n_fs, 2), dma(), dma(n_fs),
+            dma(3), dma(n_sp, n_fs), dma(2, n_sp), dma(2), dma(3), dma(3), dma(), dma(),
+            dma(), dma(n_fs), dma(), dma(), dma(), dma(2, n_fs, 2), dma(), dma(2, 2), dma(), dma(),
+            dma(), dma(), dma(n_sp, 2), dma(), dma(n_half, 2), dma(), dma(),
+        ],
+        1, "layer", [pl.BlockSpec(memory_space=pl.ANY)] * len(args),
+    )(*args)
+    return final[None]
+
+
+def run(n_sp, n_fs, n_tp, *args):
+    wr, width = args[2].shape
+    whole = n_fs * wr % 128 == 0 and args[-1].shape[1] % 128 == 0 and args[0].shape[1] % 256 == 0
+    return (fused if whole and width == n_fs * HEAD_DIM else body)(n_sp, n_fs, n_tp, *args)
+
+
 def solution(mesh):
     sizes = dict(mesh.shape)
     weight = P(("sp", "fs"), "tp")
@@ -598,6 +1257,6 @@
         P("fs", "sp", "tp"), P("tp"), P(), P("tp"), P("tp", ("sp", "fs")), P("tp", ("sp", "fs")),
     )
     return jax.shard_map(
-        functools.partial(body, sizes["sp"], sizes["fs"], sizes["tp"]),
+        functools.partial(run, sizes["sp"], sizes["fs"], sizes["tp"]),
         mesh=mesh, in_specs=placed, out_specs=P("fs", ("sp", "tp"), None), check_vma=False,
     )

time: 122 us -> 81.3 us (0.67)
  the two profiles are of different devices: /device:TPU:1 before, /device:TPU:21 now
where the time goes in v3:
time: 81.3 us; the launch traced here: 81.1 us
  Pallas kernels  77.7 us (96%)
  local copies, waits for them, and re-layouts  3.37 us (4%)
    pallas_call x1, Pallas kernels, fused(): comm(functools.partial(layer_kernel, n_sp, n_fs, n_tp), [((rows // n_tp,...  77.7 us
    unnamed x4, local copies, waits for them, and re-layouts  3.37 us

profile of v3, /device:TPU:21, one launch (start us, length us, event | category | flops | bytes accessed | tf_op | source)
XLA Modules:
  0.0 81.1 jit_solution(12690274502322813118)
XLA Ops:
  0.0 0.0 copy-start
  0.0 0.7 copy-done
  0.7 0.8 copy.15
  1.5 77.7 %layer.1 = bf16[128,2048]{1,0:T(8,128)(2,1)} custom-call(bf16[256,1024]{1,0:T(8,128)(2,1)} %bitcast.9, bf16[128,512]{1,0:T(8,128)(2,1)} %wq.1, bf16[128,512]{1,0:T(8,128)(2,1)} %wf.1, bf16[128,512]{1,0:T(8,128)(2,1)} %wi.1, bf16[128,512]{1,0:T(8,128)(2,1)} %wo.1, bf16[128,512]{1,0:T(8,128)(2,1)} %wp.1, f32[256,4]{1,0:T(8,128)} %bitcast.8, ...), custom_call_target="tpu_custom_call" | custom-call | tf_op jit(solution)/shard_map/layer/pallas_call | solution.py:1216
  79.2 1.9 %copy.17 = bf16[1,128,2048]{2,1,0:T(8,128)(2,1)} copy(bf16[1,128,2048]{2,1,0:T(8,128)(2,1)} %bitcast.7) | data formatting | bytes 1048576
Async XLA Ops:
  0.0 0.7 copy-start

commit v4 on v3

--- a/solution.py
+++ b/solution.py
@@ -521,15 +521,14 @@
     return pltpu.SemaphoreType.DMA(shape) if shape else pltpu.SemaphoreType.DMA
 
 
-def comm(kernel, outs, scratch, number, name, ins=None):
+def comm(kernel, outs, scratch, number, name, ins=None, limit=60):
     return pl.pallas_call(
         kernel,
-        out_shape=[jax.ShapeDtypeStruct(a, b) for a, b in outs],
-        out_specs=vmem(len(outs)),
-        **({} if ins is None else {"in_specs": ins}),
+        out_shape=[jax.ShapeDtypeStruct(a, b) if ins is None else pltpu.VMEM(a, b) for a, b in outs],
+        **({"out_specs": vmem(len(outs))} if ins is None else {"in_specs": ins, "out_specs": [pl.BlockSpec(memory_space=pltpu.VMEM)] * len(outs)}),
         scratch_shapes=scratch,
         compiler_params=pltpu.CompilerParams(
-            collective_id=number, has_side_effects=True, vmem_limit_bytes=60 * 1024 * 1024
+            collective_id=number, has_side_effects=True, vmem_limit_bytes=limit * 1024 * 1024
         ),
         name=name,
     )
@@ -848,9 +847,8 @@
     when(has_down, ow_down(s, 0))
     for c in loads:
         c.wait()
-    e_rows = extra[...].T
     for g in range(n_fs):
-        e_src[g] = jnp.broadcast_to(e_rows[g : g + 1, :], e_src.shape[1:])
+        e_src[g] = jnp.broadcast_to(extra[g : g + 1, :], e_src.shape[1:])
     for g in order[1:]:
         rcopy(e_src.at[g], e_all.at[f], e_send, e_recv, (s, g, t)).start()
     for c in (1, 2):
@@ -1147,6 +1145,7 @@
         came(ow_oth.at[i, k], od_recv.at[i, k])
         return t * n_half + i, i
 
+    owns = []
     for j in range(n_half):
         if j == 0:
             for k in range(2):
@@ -1164,10 +1163,14 @@
             a, i = ow_got(j, 1)
             for h in range(2):
                 pool_side(a, i, h)
-        final[:, spot_of(a, f)] = part[at_part(i, f, t)]
+        own = pltpu.make_async_copy(part.at[at_part(i, f, t)], final.at[:, spot_of(a, f)], in_sem.at[min(j, 1)])
+        own.start()
+        owns.append(own)
 
     pieces = part.at[0 : n_half * (n_tp * n_fs - 1)]
     came(pieces, m_recv)
+    for own in owns:
+        own.wait()
     sent(pieces, m_send)
     sent(xs.at[0:3, :, 0:half], x_send)
     sent(xs.at[:, :, 0:half], xd_send)
@@ -1209,7 +1212,7 @@
         return pltpu.VMEM(shape, kind)
 
     args = (
-        tokens[0], w_query, forget_weight, w_input, w_outgate, w_pool, extra_decay[0], norm_gain[None],
+        tokens[0], w_query, forget_weight, w_input, w_outgate, w_pool, extra_decay[0].T, norm_gain[None],
         forget_gap[None], rec_gain[None], group_weight, pool_gain[None], recurrent_output_weight, w_out_pool,
     )
     extra, gain, gap, r_gain, gmap, pgain = args[6:12]
@@ -1238,7 +1241,7 @@
             dma(), dma(n_fs), dma(), dma(), dma(), dma(2, n_fs, 2), dma(), dma(2, 2), dma(), dma(),
             dma(), dma(), dma(n_sp, 2), dma(), dma(n_half, 2), dma(), dma(),
         ],
-        1, "layer", [pl.BlockSpec(memory_space=pl.ANY)] * len(args),
+        1, "layer", [pl.BlockSpec(memory_space=pltpu.HBM)] * len(args), 58,
     )(*args)
     return final[None]
 

time: 81.3 us -> 77.9 us (0.958)
  local copies, waits for them, and re-layouts: 3.37 us -> 0.8 us
    unnamed x4 -> x1, local copies, waits for them, and re-layouts: 3.37 us -> 0.8 us
where the time goes in v4:
time: 77.9 us; the launch traced here: 77.7 us
  Pallas kernels  76.9 us (99%)
  local copies, waits for them, and re-layouts  0.8 us (1%)
    pallas_call x1, Pallas kernels, fused(): comm(functools.partial(layer_kernel, n_sp, n_fs, n_tp), [((rows // n_tp,...  76.9 us

profile of v4, /device:TPU:21, one launch (start us, length us, event | category | flops | bytes accessed | tf_op | source)
XLA Modules:
  0.0 77.7 jit_solution(5790011228683751057)
XLA Ops:
  0.0 76.9 %layer.1 = bf16[128,2048]{1,0:T(8,128)(2,1)S(1)} custom-call(bf16[256,1024]{1,0:T(8,128)(2,1)} %bitcast.10, bf16[128,512]{1,0:T(8,128)(2,1)} %wq.1, bf16[128,512]{1,0:T(8,128)(2,1)} %wf.1, bf16[128,512]{1,0:T(8,128)(2,1)} %wi.1, bf16[128,512]{1,0:T(8,128)(2,1)} %wo.1, bf16[128,512]{1,0:T(8,128)(2,1)} %wp.1, f32[4,256]{1,0:T(4,128)} %bitcast.12, ...), custom_call_target="tpu_custom_call" | custom-call | tf_op jit(solution)/shard_map/layer/pallas_call | solution.py:1219
  76.9 0.8 %copy.16 = bf16[1,128,2048]{2,1,0:T(8,128)(2,1)} copy(bf16[1,128,2048]{2,1,0:T(8,128)(2,1)S(1)} %bitcast.9) | data formatting | bytes 1048576

commit v5 on v4

--- a/solution.py
+++ b/solution.py
@@ -599,7 +599,7 @@
 
 def layer_kernel(
     n_sp, n_fs, n_tp, tok, wq, wf, wi, wo, wp, extra_in, gain_in, gap_in, rec_gain_in, gmap_in, pgain_in, wor, wop_in, final,
-    src0, src1, src2, ws0, ws1, ws2, xs, xn, acc0, acc1, acc2, e_src, e_all, local, qd, own_st, own_de,
+    src0, src1, src2, src3, ws0, ws1, ws2, ws3, xs, xn, acc0, acc1, acc2, acc3, k_buf, rel, st_buf, lead, e_src, e_all, local, qd, own_st, own_de,
     t_out, t_in, rim_src, rim, acts, sq_src, sq_all, ow_buf, ow_oth, part, half_way,
     extra, gain, gap, rec_gain, gmap, pgain, wop,
     in_sem, w_in, p_in, x_send, x_recv, xd_send, xd_recv, w_send, w_recv, b_recv, ba_recv, up_send, dn_send, e_send, e_recv,
@@ -618,8 +618,8 @@
     size = 128
     blk = n_fs * wr
     total_k = n_sp * blk
-    groups = ((wq, wf, wi), (wp,), (wo,))
-    srcs, wss, accs = (src0, src1, src2), (ws0, ws1, ws2), (acc0, acc1, acc2)
+    groups = ((wf, wi), (wp,), (wo,), (wq,))
+    srcs, wss, accs = (src0, src1, src2, src3), (ws0, ws1, ws2, ws3), (acc0, acc1, acc2, acc3)
     other = (s, f, 1 - t)
     px, py, pd = square(f)
     order = (f, px, py, pd)
@@ -657,7 +657,8 @@
     peers = (
         [(None, other)]
         + [(None, (s, g, u)) for g in order[1:] for u in (t, 1 - t)]
-        + [(has_up, up), (has_down, down)]
+        + [(has_up, (s + 1, f, u)) for u in (t, 1 - t)]
+        + [(has_down, (s - 1, f, u)) for u in (t, 1 - t)]
     )
     barrier = pltpu.get_barrier_semaphore()
     for cond, dev in peers:
@@ -667,7 +668,7 @@
             tell()
         else:
             pl.when(cond)(tell)
-    for c in range(3):
+    for c in (1, 0, 3, 2):
         for i, w in enumerate(groups[c]):
             for j, g in enumerate(order):
                 lane = pl.ds(pl.multiple_of(g * ch, ch), ch)
@@ -706,12 +707,23 @@
             rsem = w_recv.at[s, f] if c == 0 else ba_recv.at[c - 1]
             rcopy(srcs[c].at[j], slot(c, s, f), w_send.at[c], rsem, (s, g, t)).start()
 
-    def own_block(c):
+    def chunk(c, g, dev):
+        here = slot(c, s, g)
+        return rcopy(here, here, (up_send if dev is up else dn_send).at[c], b_recv.at[c - 1, s], dev)
+
+    def own_wait(c):
         came(wss[c].at[0 : (n_fs - 1) * wr, :], ba_recv.at[c - 1])
-        when(has_up, b_up(c, s))
-        when(has_down, b_down(c, s))
+
+    def own_up(c, cond=True):
+        when(has_up & cond, *(chunk(c, g, up) for g in order[1:]))
+
+    def own_down(c, cond=True):
+        when(has_down & cond, *(chunk(c, g, down) for g in order[1:]))
 
     low = 2 * s < n_sp
+    inner = jnp.logical_not(is_end)
+    mid_low = inner & low
+    mid_high = inner & jnp.logical_not(low)
 
     def relay(c, d, gs=(None,)):
         a, b = s - d, s + d
@@ -804,58 +816,73 @@
         i = lax.rem(a, n_half)
         when(a // n_half != t, rcopy(ow_buf.at[a, k], ow_oth.at[i, k], od_send, od_recv.at[i, k], other))
 
-    def ow_relay(d, k):
-        a, b = s - d, s + d
-
-        @pl.when((a >= 0) & has_up)
+    def ow_start(a, k, rise, cond=True):
+        to, has, edge_at = (s + 1, has_up, n_sp - 1) if rise else (s - 1, has_down, 0)
+        ssem = ou_send if rise else on_send
+        across = (to == edge_at) & (a // n_half != t)
+        i = lax.rem(a, n_half)
+        when(has & cond & jnp.logical_not(across), (ow_up if rise else ow_down)(a, k))
+        when(has & cond & across, rcopy(ow_buf.at[a, k], ow_oth.at[i, k], ssem, od_recv.at[i, k], (to, f, 1 - t)))
+
+    def ow_rise(d, k, cond=True):
+        a = s - d
+
+        @pl.when((a >= 0) & has_up & cond)
         def _():
             ow_up(a, k).wait_recv()
-            ow_up(a, k).start()
+            ow_start(a, k, True)
             ow_share(a, k)
 
-        @pl.when((b < n_sp) & has_down)
+    def ow_fall(d, k, cond=True):
+        b = s + d
+
+        @pl.when((b < n_sp) & has_down & cond)
         def _():
             ow_down(b, k).wait_recv()
-            ow_down(b, k).start()
+            ow_start(b, k, False)
             ow_share(b, k)
+
+    def ow_relay(d, k):
+        ow_rise(d, k)
+        ow_fall(d, k)
 
     def ow_take(d, k):
         a, b = s - d, s + d
-
-        @pl.when((a >= 0) & jnp.logical_not(has_up))
-        def _():
-            ow_up(a, k).wait_recv()
-            ow_share(a, k)
-
-        @pl.when((b < n_sp) & jnp.logical_not(has_down))
-        def _():
-            ow_down(b, k).wait_recv()
-            ow_share(b, k)
-
+        pl.when((a >= 0) & jnp.logical_not(has_up) & (a // n_half == t))(ow_up(a, k).wait_recv)
+        pl.when((b < n_sp) & jnp.logical_not(has_down) & (b // n_half == t))(ow_down(b, k).wait_recv)
+
+    took(slot(1, s, f), w_in.at[1, 0])
+    when(has_up, chunk(1, f, up))
+    when(has_down, chunk(1, f, down))
+    took(srcs[1], w_in.at[1, 1])
+    spread(1)
     took(slot(0, s, f), w_in.at[0, 0])
     both(s, f)
     took(srcs[0], w_in.at[0, 1])
     spread(0)
+    for c in (3, 2):
+        took(slot(c, s, f), w_in.at[c, 0])
+        when(has_up, chunk(c, f, up))
+        when(has_down, chunk(c, f, down))
     took(xs.at[f, :, cols(t)], in_sem.at[0])
     for p, hs in ((px, (0, 1)), (py, (1, 0))):
         for h in hs:
             rcopy(x_slot(f, h, t), x_slot(f, h, t), x_send, x_recv.at[f, h], (s, p, t)).start()
     for h in range(2):
         hand_on(f, h)
-    took(ow_buf.at[s, 0], in_sem.at[1])
-    when(has_up, ow_up(s, 0))
-    when(has_down, ow_down(s, 0))
     for c in loads:
         c.wait()
     for g in range(n_fs):
         e_src[g] = jnp.broadcast_to(extra[g : g + 1, :], e_src.shape[1:])
     for g in order[1:]:
         rcopy(e_src.at[g], e_all.at[f], e_send, e_recv, (s, g, t)).start()
-    for c in (1, 2):
-        took(slot(c, s, f), w_in.at[c, 0])
+    for c in (3, 2):
         took(srcs[c], w_in.at[c, 1])
         spread(c)
     e_all[f] = e_src[f]
+    own_wait(1)
+    own_up(1)
+    own_down(1)
     for g in order[1:]:
         came(slot(0, s, g), w_recv.at[s, g])
         both(s, g)
@@ -865,32 +892,43 @@
         scaled = (gmap[t * (width // gd) + i].astype(F32) * pgain[:, at]).astype(BF)
         ow_buf[s, 1, at, :] = jnp.dot(scaled, wop[at, :], preferred_element_type=F32).astype(BF)
     norm(0)
+    relay(1, 1)
     relay(0, 1, order[:2])
     for g, h, onto in ((px, 0, py), (py, 1, px)):
         here = landed(g, h)
         rcopy(here, here, x_send, x_recv.at[g, h], (s, onto, t)).start()
         hand_on(g, h)
+    for d in range(2, n_sp - 1):
+        relay(1, d)
     relay(0, 1, order[2:])
-    for d in range(2, n_sp - 1):
-        relay(0, d, order[:2])
     for g, h in ((px, 1), (py, 0)):
         landed(g, h)
         hand_on(g, h)
+    for d in range(2, n_sp - 1):
+        relay(0, d, order[:2])
     norm(1)
+    for c in (3, 2):
+        own_wait(c)
+        own_up(c, is_end)
+        own_down(c, is_end)
+    took(ow_buf.at[s, 0], in_sem.at[1])
+    for k in range(2):
+        ow_start(s, k, True, is_end)
+        ow_start(s, k, False, is_end)
+        ow_share(s, k)
+    norm(2)
+    for d in range(1, n_sp):
+        arrive(1, d)
+    gemm(1, 0, slice(0, total_k), False)
     for d in range(2, n_sp - 1):
         relay(0, d, order[2:])
-    own_block(1)
-    pl.when(is_end)(lambda: own_block(2))
-    norm(2)
-    for d in range(1, n_sp - 1):
-        arrive(0, d)
-    main(0, 0)
+    own_up(3, inner)
+    own_down(3, inner)
     for h in range(2):
         landed(pd, h)
         hand_on(pd, h)
     norm(3)
-    main(0, 1)
-    relay(1, 1)
+    gemm(1, 1, slice(0, total_k), False)
 
     reach = rim.shape[1]
     edge = rcopy(rim_src, rim, g_send, g_recv, up)
@@ -900,70 +938,11 @@
             rim_src[j] = acc1[j // 2, (j % 2 + 1) * rows - reach : (j % 2 + 1) * rows, :].astype(BF)
         when(has_up, edge)
 
-    last(0)
-    came(e_all.at[0 : n_fs - 1], e_recv)
-
-    mine = pl.ds(pl.multiple_of(f * ch, ch), ch)
-    gap_f = gap[:, mine]
-    gain_f = rec_gain[:, mine]
-    at = lax.broadcasted_iota(jnp.int32, (size, size), 0)
-    causal = at >= lax.broadcasted_iota(jnp.int32, (size, size), 1)
-    lower = jnp.where(causal, 1.0, 0.0).astype(BF)
-    lower = jnp.concatenate([lower, lower], axis=1)
-
-    def scan(j):
-        p, base = j // 2, j % 2 * rows
-        state = None
-        so_far = jnp.zeros((1, ch), F32)
-        e_cols = e_all[order[j]].T
-        for n in range(rows // size):
-            here = slice(n * size, (n + 1) * size)
-            there = slice(base + n * size, base + (n + 1) * size)
-            v = acc0[p, there, 2 * ch : 3 * ch].astype(BF)
-            q = jax.nn.silu(acc0[p, there, 0:ch].astype(BF).astype(F32))
-            k = gap_f * jax.nn.sigmoid(-acc0[p, there, ch : 2 * ch].astype(BF).astype(F32))
-            logs = jnp.log1p(-k) + e_cols[here, 0:1]
-            high = logs.astype(BF)
-            low = (logs - high.astype(F32)).astype(BF)
-            within = mm(lower, jnp.concatenate([high, low], axis=0), NN)
-            mid = within[size // 2 - 1 : size // 2]
-            end = within[size - 1 :]
-            q = q * jnp.exp(within - mid)
-            k = (k * jnp.exp(mid - within)).astype(BF)
-            q_up = q.astype(BF)
-            scores = jnp.where(causal, mm(q_up, k, NT), 0.0).astype(BF)
-            out = mm(scores, v, NN)
-            if n:
-                out = out + mm(q_up, (state * jnp.exp(mid)).astype(BF), NT)
-            local[j, here, :] = out
-            qd[j, here, :] = (q * jnp.exp(mid + so_far)).astype(BF)
-            fresh = mm(v, k, TN) * jnp.exp(end - mid)
-            state = state * jnp.exp(end) + fresh if n else fresh
-            so_far = so_far + end
-        own_st[j] = state
-        own_de[j] = jnp.broadcast_to(jnp.exp(so_far), own_de.shape[1:])
-
-    def carry(g):
-        return rcopy(t_out.at[g], t_in.at[g], t_send, t_recv.at[g], up)
-
-    for j in range(n_fs):
-        scan(j)
-
-        @pl.when(jnp.logical_not(has_down))
-        def _():
-            t_in[j] = jnp.zeros(t_in.shape[1:], BF)
-            t_out[j] = own_st[j].astype(BF)
-            carry(j).start()
-
-    for d in range(2, n_sp - 1):
-        relay(1, d)
-    pl.when(jnp.logical_not(is_end))(lambda: own_block(2))
-    @pl.when(jnp.logical_not(is_end))
-    def _():
-        each_pair(lambda p: gemm(1, p, slice(0, total_k), False))
-        send_rim()
-
-    relay(2, 1)
+    send_rim()
+    relay(3, 1)
+    for d in range(1, n_sp - 1):
+        arrive(0, d)
+    each_pair(lambda p: main(0, p))
     def chain():
         for g in range(n_fs):
             carry(g).wait_recv()
@@ -1029,32 +1008,103 @@
             pool(j)
         publish(1)
 
-    mid_low = jnp.logical_not(is_end) & low
-    mid_high = jnp.logical_not(is_end) & jnp.logical_not(low)
+    @pl.when(jnp.logical_not(has_down))
+    def _():
+        rim[...] = jnp.zeros(rim.shape, BF)
+
+    pool_all()
+    last(0)
+    came(e_all.at[0 : n_fs - 1], e_recv)
+
+    mine = pl.ds(pl.multiple_of(f * ch, ch), ch)
+    gap_f = gap[:, mine]
+    gain_f = rec_gain[:, mine]
+    at = lax.broadcasted_iota(jnp.int32, (size, size), 0)
+    causal = at >= lax.broadcasted_iota(jnp.int32, (size, size), 1)
+    lower = jnp.where(causal, 1.0, 0.0).astype(BF)
+    lower = jnp.concatenate([lower, lower], axis=1)
+
+    steps = rows // size
+
+    def spots(j, n):
+        lo = j % 2 * rows + n * size
+        return slice(n * size, (n + 1) * size), slice(lo, lo + size)
+
+    def states(j):
+        state = None
+        so_far = jnp.zeros((1, ch), F32)
+        e_cols = e_all[order[j]].T
+        for n in range(steps):
+            here, there = spots(j, n)
+            v = acc0[j // 2, there, ch : 2 * ch].astype(BF)
+            k = gap_f * jax.nn.sigmoid(-acc0[j // 2, there, 0:ch].astype(BF).astype(F32))
+            logs = jnp.log1p(-k) + e_cols[here, 0:1]
+            high = logs.astype(BF)
+            low = (logs - high.astype(F32)).astype(BF)
+            within = mm(lower, jnp.concatenate([high, low], axis=0), NN)
+            mid = within[size // 2 - 1 : size // 2]
+            end = within[size - 1 :]
+            k = (k * jnp.exp(mid - within)).astype(BF)
+            k_buf[j, here, :] = k
+            rel[j, here, :] = within - mid
+            lead[j, n] = jnp.broadcast_to(jnp.exp(mid + so_far), lead.shape[2:])
+            fresh = mm(v, k, TN) * jnp.exp(end - mid)
+            if n:
+                st_buf[j, n - 1] = (state * jnp.exp(mid)).astype(BF)
+            state = state * jnp.exp(end) + fresh if n else fresh
+            so_far = so_far + end
+        own_st[j] = state
+        own_de[j] = jnp.broadcast_to(jnp.exp(so_far), own_de.shape[1:])
+
+    def reads(j):
+        for n in range(steps):
+            here, there = spots(j, n)
+            v = acc0[j // 2, there, ch : 2 * ch].astype(BF)
+            q = jax.nn.silu(acc3[j // 2, there, :].astype(BF).astype(F32)) * jnp.exp(rel[j, here, :])
+            q_up = q.astype(BF)
+            scores = jnp.where(causal, mm(q_up, k_buf[j, here, :], NT), 0.0).astype(BF)
+            out = mm(scores, v, NN)
+            if n:
+                out = out + mm(q_up, st_buf[j, n - 1], NT)
+            local[j, here, :] = out
+            qd[j, here, :] = (q * lead[j, n, 0:1, :]).astype(BF)
+
+    def carry(g):
+        return rcopy(t_out.at[g], t_in.at[g], t_send, t_recv.at[g], up)
+
+    for j in range(n_fs):
+        states(j)
+
+        @pl.when(jnp.logical_not(has_down))
+        def _():
+            t_in[j] = jnp.zeros(t_in.shape[1:], BF)
+            t_out[j] = own_st[j].astype(BF)
+            carry(j).start()
+
+    for d in range(2, n_sp - 1):
+        relay(3, d)
+    own_up(2, inner)
+    own_down(2, inner)
+    for d in range(1, n_sp - 1):
+        arrive(3, d)
+    each_pair(lambda p: main(3, p))
+    last(3)
+    for j in range(n_fs):
+        reads(j)
+    relay(2, 1)
     pl.when(mid_low)(chain)
     for d in range(2, n_sp - 1):
         relay(2, d)
-    pl.when(jnp.logical_not(is_end))(lambda: each_pair(lambda p: gemm(2, p, slice(0, total_k), False)))
-    pl.when(mid_high)(pool_all)
+    for k in range(2):
+        ow_start(s, k, False, inner)
+    a_forward(1, 0)
     pl.when(mid_high)(chain)
-    when(has_up, ow_up(s, 1))
-    when(has_down, ow_down(s, 1))
     for k in range(2):
-        ow_share(s, k)
-    ow_relay(1, 0)
-    for d in range(1, n_sp - 1):
-        arrive(1, d)
-    pl.when(is_end)(lambda: each_pair(lambda p: gemm(1, p, near, False)))
-    last(1)
-    @pl.when(is_end)
-    def _():
-        send_rim()
-
-        @pl.when(jnp.logical_not(has_down))
-        def _():
-            rim[...] = jnp.zeros(rim.shape, BF)
-
-    pl.when(jnp.logical_not(mid_high))(pool_all)
+        ow_start(s, k, True, inner)
+        ow_rise(1, k, mid_low)
+        ow_fall(1, k, mid_high)
+    pl.when(inner)(lambda: each_pair(lambda p: gemm(2, p, slice(0, total_k), False)))
+    a_forward(1, 1)
     ones = jnp.ones((8, ch), BF)
 
     def finish(j):
@@ -1074,13 +1124,16 @@
         publish(0)
         sq_all[t * n_fs + f] = sq_src[...]
 
-    pl.when(jnp.logical_not(is_end))(finish_all)
+    pl.when(inner)(finish_all)
+    for k in range(2):
+        ow_rise(1, k, mid_high)
+    pl.when(inner)(lambda: a_forward(0, 0))
+    for k in range(2):
+        ow_fall(1, k, mid_low)
+    pl.when(inner)(lambda: a_forward(0, 1))
     for d in range(1, n_sp - 1):
         arrive(2, d)
     pl.when(is_end)(lambda: each_pair(lambda p: gemm(2, p, near, False)))
-    a_forward(1, 0)
-    ow_relay(1, 1)
-    a_forward(1, 1)
     last(2)
     @pl.when(has_down & jnp.logical_not(has_up))
     def _():
@@ -1094,8 +1147,8 @@
         a_rest(1, h)
     for d in range(2, n_sp - 1):
         ow_relay(d, 1)
-    a_forward(0, 0)
-    a_forward(0, 1)
+    pl.when(is_end)(lambda: a_forward(0, 0))
+    pl.when(is_end)(lambda: a_forward(0, 1))
     for d in range(1, n_sp - 1):
         for k in range(2):
             ow_take(d, k)
@@ -1175,23 +1228,24 @@
     sent(xs.at[0:3, :, 0:half], x_send)
     sent(xs.at[:, :, 0:half], xd_send)
     sent(e_src.at[0 : n_fs - 1], e_send)
-    for c in range(3):
+    for c in range(4):
         sent(srcs[c], w_send.at[c])
     sent(acts.at[:, 0, 0:3], a_send)
     sent(acts.at[:, 0], ad_send)
     sent(sq_all.at[0 : n_tp * n_fs - 1], q_send)
-    sent(ow_oth, od_send)
+    pl.when(jnp.logical_not(is_end))(lambda: sent(ow_oth, od_send))
+    pl.when(is_end & (s // n_half != t))(lambda: sent(ow_oth.at[0], od_send))
     for v in range(n_sp):
         @pl.when(s == v)
         def _():
             if v < n_sp - 1:
-                for c in range(3):
+                for c in range(4):
                     sent(wss[c].at[0 : (v + 1) * blk, :], up_send.at[c])
                 sent(ow_buf.at[0 : v + 1], ou_send)
                 sent(rim_src, g_send)
                 sent(t_out, t_send)
             if v > 0:
-                for c in range(3):
+                for c in range(4):
                     sent(wss[c].at[0 : (n_sp - v) * blk, :], dn_send.at[c])
                 sent(ow_buf.at[0 : n_sp - v], on_send)
 
@@ -1220,10 +1274,12 @@
         functools.partial(layer_kernel, n_sp, n_fs, n_tp),
         [((rows // n_tp, n_sp * n_fs * cw), BF)],
         [
-            buf(BF, n_fs - 1, wr, 3 * ch), buf(BF, n_fs - 1, wr, ch), buf(BF, n_fs - 1, wr, ch),
-            buf(BF, feats, 3 * ch), buf(BF, feats, ch), buf(BF, feats, ch),
+            buf(BF, n_fs - 1, wr, 2 * ch), buf(BF, n_fs - 1, wr, ch), buf(BF, n_fs - 1, wr, ch), buf(BF, n_fs - 1, wr, ch),
+            buf(BF, feats, 2 * ch), buf(BF, feats, ch), buf(BF, feats, ch), buf(BF, feats, ch),
             buf(BF, n_fs, rows, n_tp * half), buf(BF, 2, n_fs // 2 * rows, n_tp * half),
-            buf(F32, 2, n_fs // 2 * rows, 3 * ch), buf(F32, 2, n_fs // 2 * rows, ch), buf(F32, 2, n_fs // 2 * rows, ch),
+            buf(F32, 2, n_fs // 2 * rows, 2 * ch), buf(F32, 2, n_fs // 2 * rows, ch), buf(F32, 2, n_fs // 2 * rows, ch),
+            buf(F32, 2, n_fs // 2 * rows, ch), buf(BF, n_fs, rows, ch), buf(F32, n_fs, rows, ch),
+            buf(BF, n_fs, rows // 128, ch, ch), buf(F32, n_fs, rows // 128, 8, ch),
             buf(F32, n_fs, 8, rows), buf(F32, n_fs, 8, rows),
             buf(F32, n_fs, rows, ch), buf(BF, n_fs, rows, ch),
             buf(F32, n_fs, ch, ch), buf(F32, n_fs, 8, ch),
@@ -1236,8 +1292,8 @@
         ]
         + [buf(a.dtype, *a.shape) for a in (extra, gain, gap, r_gain, gmap, pgain, w_out_pool)]
         + [
-            dma(2), dma(3, 2), dma(7), dma(), dma(n_fs, 2), dma(), dma(n_fs),
-            dma(3), dma(n_sp, n_fs), dma(2, n_sp), dma(2), dma(3), dma(3), dma(), dma(),
+            dma(2), dma(4, 2), dma(7), dma(), dma(n_fs, 2), dma(), dma(n_fs),
+            dma(4), dma(n_sp, n_fs), dma(3, n_sp), dma(3), dma(4), dma(4), dma(), dma(),
             dma(), dma(n_fs), dma(), dma(), dma(), dma(2, n_fs, 2), dma(), dma(2, 2), dma(), dma(),
             dma(), dma(), dma(n_sp, 2), dma(), dma(n_half, 2), dma(), dma(),
         ],

time: 77.9 us -> 75.7 us (0.972)
  the two profiles are of different devices: /device:TPU:21 before, /device:TPU:29 now
where the time goes in v5:
time: 75.7 us; the launch traced here: 75.6 us
  Pallas kernels  74.8 us (99%)
  local copies, waits for them, and re-layouts  0.8 us (1%)
    pallas_call x1, Pallas kernels, fused(): comm(functools.partial(layer_kernel, n_sp, n_fs, n_tp), [((rows // n_tp,...  74.8 us

profile of v5, /device:TPU:29, one launch (start us, length us, event | category | flops | bytes accessed | tf_op | source)
XLA Modules:
  0.0 75.6 jit_solution(10765562279245654372)
XLA Ops:
  0.0 74.8 %layer.1 = bf16[128,2048]{1,0:T(8,128)(2,1)S(1)} custom-call(bf16[256,1024]{1,0:T(8,128)(2,1)} %bitcast.10, bf16[128,512]{1,0:T(8,128)(2,1)} %wq.1, bf16[128,512]{1,0:T(8,128)(2,1)} %wf.1, bf16[128,512]{1,0:T(8,128)(2,1)} %wi.1, bf16[128,512]{1,0:T(8,128)(2,1)} %wo.1, bf16[128,512]{1,0:T(8,128)(2,1)} %wp.1, f32[4,256]{1,0:T(4,128)} %bitcast.12, ...), custom_call_target="tpu_custom_call" | custom-call | tf_op jit(solution)/shard_map/layer/pallas_call | solution.py:1273
  74.8 0.8 %copy.16 = bf16[1,128,2048]{2,1,0:T(8,128)(2,1)} copy(bf16[1,128,2048]{2,1,0:T(8,128)(2,1)S(1)} %bitcast.9) | data formatting | bytes 1048576

commit v6 on v5

--- a/solution.py
+++ b/solution.py
@@ -604,7 +604,7 @@
     extra, gain, gap, rec_gain, gmap, pgain, wop,
     in_sem, w_in, p_in, x_send, x_recv, xd_send, xd_recv, w_send, w_recv, b_recv, ba_recv, up_send, dn_send, e_send, e_recv,
     t_send, t_recv, g_send, g_recv, a_send, a_recv, ad_send, ad_recv, q_send, q_recv,
-    ou_send, on_send, o_recv, od_send, od_recv, m_send, m_recv,
+    ou_send, on_send, o_recv, od_send, od_recv, m_send, m_recv, ready,
 ):
     s, f, t = place()
     rows, half = tok.shape
@@ -656,9 +656,8 @@
 
     peers = (
         [(None, other)]
-        + [(None, (s, g, u)) for g in order[1:] for u in (t, 1 - t)]
-        + [(has_up, (s + 1, f, u)) for u in (t, 1 - t)]
-        + [(has_down, (s - 1, f, u)) for u in (t, 1 - t)]
+        + [(None, (s, px, t)), (None, (s, py, t))]
+        + [(has_up, up), (has_down, down)]
     )
     barrier = pltpu.get_barrier_semaphore()
     for cond, dev in peers:
@@ -702,8 +701,9 @@
     def b_down(c, a):
         return rcopy(block(c, a), block(c, a), dn_send.at[c], b_recv.at[c - 1, a], down)
 
-    def spread(c):
-        for j, g in enumerate(order[1:]):
+    def spread(c, some=(0, 1, 2)):
+        for j in some:
+            g = order[1 + j]
             rsem = w_recv.at[s, f] if c == 0 else ba_recv.at[c - 1]
             rcopy(srcs[c].at[j], slot(c, s, f), w_send.at[c], rsem, (s, g, t)).start()
 
@@ -725,7 +725,7 @@
     mid_low = inner & low
     mid_high = inner & jnp.logical_not(low)
 
-    def relay(c, d, gs=(None,)):
+    def relay(c, d, gs=(None,), inward=True, outward=True):
         a, b = s - d, s + d
 
         def rising(extra):
@@ -736,17 +736,20 @@
                     hop.wait_recv()
                     hop.start()
 
-        def falling():
+        def falling(extra):
             for g in gs:
-                @pl.when((b < n_sp) & has_down)
+                @pl.when((b < n_sp) & has_down & extra)
                 def _():
                     hop = to_down(slot(0, b, g), g, b) if c == 0 else b_down(c, b)
                     hop.wait_recv()
                     hop.start()
 
-        rising(low)
-        falling()
-        rising(jnp.logical_not(low))
+        if inward:
+            rising(low)
+            falling(jnp.logical_not(low))
+        if outward:
+            falling(low)
+            rising(jnp.logical_not(low))
 
     def arrive(c, d):
         for g in order if c == 0 else (None,):
@@ -851,19 +854,23 @@
         pl.when((a >= 0) & jnp.logical_not(has_up) & (a // n_half == t))(ow_up(a, k).wait_recv)
         pl.when((b < n_sp) & jnp.logical_not(has_down) & (b // n_half == t))(ow_down(b, k).wait_recv)
 
+    pl.semaphore_signal(ready, inc=1, device_id=(s, px, t), device_id_type=MESH)
     took(slot(1, s, f), w_in.at[1, 0])
     when(has_up, chunk(1, f, up))
     when(has_down, chunk(1, f, down))
     took(srcs[1], w_in.at[1, 1])
-    spread(1)
+    spread(1, (0, 1))
     took(slot(0, s, f), w_in.at[0, 0])
     both(s, f)
     took(srcs[0], w_in.at[0, 1])
-    spread(0)
+    spread(0, (0, 1))
     for c in (3, 2):
         took(slot(c, s, f), w_in.at[c, 0])
         when(has_up, chunk(c, f, up))
         when(has_down, chunk(c, f, down))
+    pl.semaphore_wait(ready, 1)
+    spread(1, (2,))
+    spread(0, (2,))
     took(xs.at[f, :, cols(t)], in_sem.at[0])
     for p, hs in ((px, (0, 1)), (py, (1, 0))):
         for h in hs:
@@ -940,6 +947,8 @@
 
     send_rim()
     relay(3, 1)
+    own_up(2, mid_low)
+    own_down(2, mid_high)
     for d in range(1, n_sp - 1):
         arrive(0, d)
     each_pair(lambda p: main(0, p))
@@ -1083,16 +1092,17 @@
 
     for d in range(2, n_sp - 1):
         relay(3, d)
-    own_up(2, inner)
-    own_down(2, inner)
+    own_up(2, mid_high)
+    own_down(2, mid_low)
+    relay(2, 1, outward=False)
     for d in range(1, n_sp - 1):
         arrive(3, d)
     each_pair(lambda p: main(3, p))
     last(3)
     for j in range(n_fs):
         reads(j)
-    relay(2, 1)
     pl.when(mid_low)(chain)
+    relay(2, 1, inward=False)
     for d in range(2, n_sp - 1):
         relay(2, d)
     for k in range(2):
@@ -1296,6 +1306,7 @@
             dma(4), dma(n_sp, n_fs), dma(3, n_sp), dma(3), dma(4), dma(4), dma(), dma(),
             dma(), dma(n_fs), dma(), dma(), dma(), dma(2, n_fs, 2), dma(), dma(2, 2), dma(), dma(),
             dma(), dma(), dma(n_sp, 2), dma(), dma(n_half, 2), dma(), dma(),
+            pltpu.SemaphoreType.REGULAR,
         ],
         1, "layer", [pl.BlockSpec(memory_space=pltpu.HBM)] * len(args), 58,
     )(*args)

time: 75.7 us -> 74.7 us (0.987)
  Pallas kernels: 74.8 us -> 73.7 us
    pallas_call x1, Pallas kernels: 74.8 us -> 73.7 us  [fused(): comm(functools.partial(layer_kernel, n_sp, n_fs, n_tp), [((rows // n_tp,...]
where the time goes in v6:
time: 74.7 us; the launch traced here: 74.5 us
  Pallas kernels  73.7 us (99%)
  local copies, waits for them, and re-layouts  0.8 us (1%)
    pallas_call x1, Pallas kernels, fused(): comm(functools.partial(layer_kernel, n_sp, n_fs, n_tp), [((rows // n_tp,...  73.7 us

profile of v6, /device:TPU:29, one launch (start us, length us, event | category | flops | bytes accessed | tf_op | source)
XLA Modules:
  0.0 74.5 jit_solution(6929703134229662174)
XLA Ops:
  0.0 73.7 %layer.1 = bf16[128,2048]{1,0:T(8,128)(2,1)S(1)} custom-call(bf16[256,1024]{1,0:T(8,128)(2,1)} %bitcast.10, bf16[128,512]{1,0:T(8,128)(2,1)} %wq.1, bf16[128,512]{1,0:T(8,128)(2,1)} %wf.1, bf16[128,512]{1,0:T(8,128)(2,1)} %wi.1, bf16[128,512]{1,0:T(8,128)(2,1)} %wo.1, bf16[128,512]{1,0:T(8,128)(2,1)} %wp.1, f32[4,256]{1,0:T(4,128)} %bitcast.12, ...), custom_call_target="tpu_custom_call" | custom-call | tf_op jit(solution)/shard_map/layer/pallas_call | solution.py:1283
  73.7 0.8 %copy.16 = bf16[1,128,2048]{2,1,0:T(8,128)(2,1)} copy(bf16[1,128,2048]{2,1,0:T(8,128)(2,1)S(1)} %bitcast.9) | data formatting | bytes 1048576

commit v7 on v6

--- a/solution.py
+++ b/solution.py
@@ -809,15 +809,19 @@
 
         lax.fori_loop(0, rows // tile, each, 0, unroll=2)
 
+    def cut_of(ref, a, k):
+        mid = width // 2
+        return ref.at[a, k // 3] if k in (0, 3) else ref.at[a, 1, (k - 1) * mid : k * mid, :]
+
     def ow_up(a, k):
-        return rcopy(ow_buf.at[a, k], ow_buf.at[a, k], ou_send, o_recv.at[a, k], up)
+        return rcopy(cut_of(ow_buf, a, k), cut_of(ow_buf, a, k), ou_send, o_recv.at[a, k], up)
 
     def ow_down(a, k):
-        return rcopy(ow_buf.at[a, k], ow_buf.at[a, k], on_send, o_recv.at[a, k], down)
+        return rcopy(cut_of(ow_buf, a, k), cut_of(ow_buf, a, k), on_send, o_recv.at[a, k], down)
 
     def ow_share(a, k):
         i = lax.rem(a, n_half)
-        when(a // n_half != t, rcopy(ow_buf.at[a, k], ow_oth.at[i, k], od_send, od_recv.at[i, k], other))
+        when(a // n_half != t, rcopy(cut_of(ow_buf, a, k), cut_of(ow_oth, i, k), od_send, od_recv.at[i, k], other))
 
     def ow_start(a, k, rise, cond=True):
         to, has, edge_at = (s + 1, has_up, n_sp - 1) if rise else (s - 1, has_down, 0)
@@ -825,7 +829,7 @@
         across = (to == edge_at) & (a // n_half != t)
         i = lax.rem(a, n_half)
         when(has & cond & jnp.logical_not(across), (ow_up if rise else ow_down)(a, k))
-        when(has & cond & across, rcopy(ow_buf.at[a, k], ow_oth.at[i, k], ssem, od_recv.at[i, k], (to, f, 1 - t)))
+        when(has & cond & across, rcopy(cut_of(ow_buf, a, k), cut_of(ow_oth, i, k), ssem, od_recv.at[i, k], (to, f, 1 - t)))
 
     def ow_rise(d, k, cond=True):
         a = s - d
@@ -919,7 +923,7 @@
         own_up(c, is_end)
         own_down(c, is_end)
     took(ow_buf.at[s, 0], in_sem.at[1])
-    for k in range(2):
+    for k in range(3):
         ow_start(s, k, True, is_end)
         ow_start(s, k, False, is_end)
         ow_share(s, k)
@@ -1105,11 +1109,11 @@
     relay(2, 1, inward=False)
     for d in range(2, n_sp - 1):
         relay(2, d)
-    for k in range(2):
+    for k in range(3):
         ow_start(s, k, False, inner)
     a_forward(1, 0)
     pl.when(mid_high)(chain)
-    for k in range(2):
+    for k in range(3):
         ow_start(s, k, True, inner)
         ow_rise(1, k, mid_low)
         ow_fall(1, k, mid_high)
@@ -1135,10 +1139,10 @@
         sq_all[t * n_fs + f] = sq_src[...]
 
     pl.when(inner)(finish_all)
-    for k in range(2):
+    for k in range(3):
         ow_rise(1, k, mid_high)
     pl.when(inner)(lambda: a_forward(0, 0))
-    for k in range(2):
+    for k in range(3):
         ow_fall(1, k, mid_low)
     pl.when(inner)(lambda: a_forward(0, 1))
     for d in range(1, n_sp - 1):
@@ -1157,10 +1161,11 @@
         a_rest(1, h)
     for d in range(2, n_sp - 1):
         ow_relay(d, 1)
+        ow_relay(d, 2)
     pl.when(is_end)(lambda: a_forward(0, 0))
     pl.when(is_end)(lambda: a_forward(0, 1))
     for d in range(1, n_sp - 1):
-        for k in range(2):
+        for k in range(3):
             ow_take(d, k)
     came(sq_all.at[0 : n_tp * n_fs - 1], q_recv)
     sums = sum(sq_all[i] for i in range(n_tp * n_fs))
@@ -1183,9 +1188,12 @@
 
     def weight_side(k, a, i, h):
         here = slice(h * part_rows, (h + 1) * part_rows)
+        side, heads = k // 3, range(n_fs)
+        if k in (1, 2):
+            side, heads = 1, range((k - 1) * n_fs // 2, k * n_fs // 2)
         total = None
-        for u, w in ((t, ow_buf.at[a, k]), (1 - t, ow_oth.at[i, k])):
-            left = jnp.concatenate([acts[k, u, b, here, :] for b in range(n_fs)], axis=1)
+        for u, w in ((t, cut_of(ow_buf, a, k)), (1 - t, cut_of(ow_oth, i, k))):
+            left = jnp.concatenate([acts[side, u, b, here, :] for b in heads], axis=1)
             now = jnp.dot(left, w[...], preferred_element_type=F32)
             total = now if total is None else total + now
         return total
@@ -1193,8 +1201,11 @@
     def rec_side(a, i, h):
         half_way[h] = weight_side(0, a, i, h) * scales[h]
 
-    def pool_side(a, i, h):
-        mixed = (half_way[h] + weight_side(1, a, i, h)).astype(BF)
+    def first_side(a, i, h):
+        half_way[h] = half_way[h] + weight_side(1, a, i, h)
+
+    def pool_side(a, i, h, k=2):
+        mixed = (half_way[h] + weight_side(k, a, i, h)).astype(BF)
         for g in range(h * n_fs // 2, (h + 1) * n_fs // 2):
             for u in range(n_tp):
                 lo = (g * n_tp + u) * out_rows - h * part_rows
@@ -1205,25 +1216,28 @@
         i = jnp.where(late, n_half - 1 - j, j)
         if j == n_half - 1:
             ow_take(n_sp - 1, k)
-        came(ow_oth.at[i, k], od_recv.at[i, k])
+        came(cut_of(ow_oth, i, k), od_recv.at[i, k])
         return t * n_half + i, i
 
     owns = []
     for j in range(n_half):
         if j == 0:
-            for k in range(2):
+            for k in range(3):
                 a, i = ow_got(0, k)
             for h in range(2):
                 a_rest(0, h)
                 for k in range(2):
                     a_other(k, h)
                 rec_side(a, i, h)
-                pool_side(a, i, h)
+                pool_side(a, i, h, 3)
         else:
             a, i = ow_got(j, 0)
             for h in range(2):
                 rec_side(a, i, h)
             a, i = ow_got(j, 1)
+            for h in range(2):
+                first_side(a, i, h)
+            a, i = ow_got(j, 2)
             for h in range(2):
                 pool_side(a, i, h)
         own = pltpu.make_async_copy(part.at[at_part(i, f, t)], final.at[:, spot_of(a, f)], in_sem.at[min(j, 1)])
@@ -1305,7 +1319,7 @@
             dma(2), dma(4, 2), dma(7), dma(), dma(n_fs, 2), dma(), dma(n_fs),
             dma(4), dma(n_sp, n_fs), dma(3, n_sp), dma(3), dma(4), dma(4), dma(), dma(),
             dma(), dma(n_fs), dma(), dma(), dma(), dma(2, n_fs, 2), dma(), dma(2, 2), dma(), dma(),
-            dma(), dma(), dma(n_sp, 2), dma(), dma(n_half, 2), dma(), dma(),
+            dma(), dma(), dma(n_sp, 3), dma(), dma(n_half, 3), dma(), dma(),
             pltpu.SemaphoreType.REGULAR,
         ],
         1, "layer", [pl.BlockSpec(memory_space=pltpu.HBM)] * len(args), 58,

time: 74.7 us -> 74.8 us (level)
  no operation moved by 1% of the time
where the time goes in v7:
time: 74.8 us; the launch traced here: 74.7 us
  Pallas kernels  73.9 us (99%)
  local copies, waits for them, and re-layouts  0.8 us (1%)
    pallas_call x1, Pallas kernels, fused(): comm(functools.partial(layer_kernel, n_sp, n_fs, n_tp), [((rows // n_tp,...  73.9 us

profile of v7, /device:TPU:29, one launch (start us, length us, event | category | flops | bytes accessed | tf_op | source)
XLA Modules:
  0.0 74.7 jit_solution(3281938892471831970)
XLA Ops:
  0.0 73.9 %layer.1 = bf16[128,2048]{1,0:T(8,128)(2,1)S(1)} custom-call(bf16[256,1024]{1,0:T(8,128)(2,1)} %bitcast.10, bf16[128,512]{1,0:T(8,128)(2,1)} %wq.1, bf16[128,512]{1,0:T(8,128)(2,1)} %wf.1, bf16[128,512]{1,0:T(8,128)(2,1)} %wi.1, bf16[128,512]{1,0:T(8,128)(2,1)} %wo.1, bf16[128,512]{1,0:T(8,128)(2,1)} %wp.1, f32[4,256]{1,0:T(4,128)} %bitcast.12, ...), custom_call_target="tpu_custom_call" | custom-call | tf_op jit(solution)/shard_map/layer/pallas_call | solution.py:1297
  73.9 0.8 %copy.16 = bf16[1,128,2048]{2,1,0:T(8,128)(2,1)} copy(bf16[1,128,2048]{2,1,0:T(8,128)(2,1)S(1)} %bitcast.9) | data formatting | bytes 1048576
